TPU v7x, 256 devices: a whole 4x4x8 slice. The times are simulated.
256 devices in a mesh: sp: 64 (over z, y, core), tp: 4 (over x).
Axes of the slice: x: 4, y: 4, z: 8, core: 2. Of those that a mesh axis runs over, the one named last changes fastest.
Arguments:
- cotangent: bfloat16 [16384, 2048], P('sp'), may hold values from -16 to 16
- stream_in: bfloat16 [16384, 2048], P('sp'), may hold values from -6 to 6
- norm_gain: float32 [2048], replicated, may hold values from 0.1 to 1.9
- out_gate: bfloat16 [16384, 1024], P('sp', 'tp'), may hold values from -6 to 6
- in_gate: bfloat16 [16384, 1024], P('sp', 'tp'), may hold values from -6 to 6
- conv_input: bfloat16 [16384, 1024], P('sp', 'tp'), may hold values from -6 to 6
- conv_taps: float32 [3, 1024], P(None, 'tp'), may hold values from -3 to 3
- out_weight: bfloat16 [2048, 1024], P(None, 'tp'), may hold values from -0.1875 to 0.1875
- expert_gate: bfloat16 [64, 2048, 1024], P('sp', None, 'tp'), may hold values from -0.125 to 0.125
- expert_up: bfloat16 [64, 2048, 1024], P('sp', None, 'tp'), may hold values from -0.125 to 0.125
- expert_down: bfloat16 [64, 1024, 2048], P('sp', 'tp'), may hold values from -0.1875 to 0.1875
- expert_choice: int32 [16384, 2], P('sp'), may hold values from 0 to 63, all different within a row; in each aligned block of 256 rows (0 to 255, 256 to 511, ...) at most 16 rows name the same one
- route_scale: float32 [16384, 2], P('sp'), may hold values from 0.05 to 0.6
Outputs:
- grad_stream: bfloat16 [16384, 2048], P('sp', 'tp')
- grad_out_gate: bfloat16 [16384, 1024], P('sp', 'tp')
- grad_in_gate: bfloat16 [16384, 1024], P('sp', 'tp')
- grad_conv_input: bfloat16 [16384, 1024], P('sp', 'tp')
- grad_out_weight: float32 [2048, 1024], P('sp', 'tp')
- grad_expert_gate: float32 [64, 2048, 1024], P('sp', None, 'tp')
- grad_expert_up: float32 [64, 2048, 1024], P('sp', None, 'tp')
- grad_expert_down: float32 [64, 1024, 2048], P('sp', 'tp')
Inputs may be any that keep to these rules, and one draw needn't show every extreme that they name: `expert_choice`: each row names two different experts. Within the rows of one device no expert is named more than 16 times, a bound that some block reaches in some devices' rows.
All inputs are finite; a program needn't handle non-finite values.
Results may differ from a plain program's by a relative error of at most 0.01.
Values may be sent and summed in bfloat16 or wider, within the bound.
A program may use at most 128 MiB of HBM per device.

v0:
```python
import jax
import jax.numpy as jnp
from jax import lax
from jax.sharding import PartitionSpec as P

norm_eps = 1e-06


def sent_together(arrays, axis, dim, along):
    widths = [a.shape[along] for a in arrays]
    both = jnp.concatenate(arrays, axis=along)
    filled = lax.all_gather(both, axis, axis=dim, tiled=True)
    return tuple(jnp.split(filled, [sum(widths[:k]) for k in range(1, len(widths))], axis=along))


def split_up(array, dim, peers):
    dims = array.shape
    tiles = array.reshape(*dims[:dim], peers, dims[dim] // peers, *dims[dim + 1 :])
    return jnp.moveaxis(tiles, dim, 0)


def sent_and_summed(array, axis, dim):
    tiles = split_up(array, dim, lax.axis_size(axis))
    arrived = lax.all_to_all(tiles, axis, split_axis=0, concat_axis=0, tiled=True)
    return arrived.astype(jnp.float32).sum(axis=0)


def passed_along(value, axis, steps):
    count = lax.axis_size(axis)
    first, last = (max(0, -steps), min(count, count - steps))
    return lax.ppermute(value, axis, [(source, source + steps) for source in range(first, last)])


def copy_for_each(array, axis):
    copies = jnp.broadcast_to(array, (lax.axis_size(axis), *array.shape))
    return lax.all_to_all(copies, axis, split_axis=0, concat_axis=0, tiled=True)


def joined_along(tiles, dim):
    tiles = jnp.moveaxis(tiles, 0, dim)
    dims = tiles.shape
    return tiles.reshape(*dims[:dim], dims[dim] * dims[dim + 1], *dims[dim + 2 :])


def gather_directly(array, axis, dim):
    tiles = copy_for_each(array, axis)
    return joined_along(tiles, dim)


def slot_table(choice_rows, expert_count, capacity):
    flat_ids = choice_rows.reshape(-1)
    route_count = flat_ids.shape[0]
    onehot = (flat_ids[:, None] == jnp.arange(expert_count, dtype=jnp.int32)[None, :]).astype(
        jnp.int32
    )
    earlier = jnp.cumsum(onehot, axis=0) - onehot
    position = jnp.sum(earlier * onehot, axis=1)
    slot_of_route = flat_ids * capacity + position
    route_of_slot = jnp.full((expert_count * capacity,), route_count, jnp.int32)
    route_of_slot = route_of_slot.at[slot_of_route].set(jnp.arange(route_count, dtype=jnp.int32))
    return (slot_of_route, route_of_slot)


def rows_product(left, right):
    return lax.dot_general(
        left, right, (((0,), (0,)), ((), ())), preferred_element_type=jnp.float32
    )


def cols_product(left, right):
    return lax.dot_general(
        left, right, (((1,), (1,)), ((), ())), preferred_element_type=jnp.float32
    )


def shards(
    cotangent,
    stream_in,
    norm_gain,
    out_gate,
    in_gate,
    conv_input,
    conv_taps,
    out_weight,
    expert_gate,
    expert_up,
    expert_down,
    expert_choice,
    route_scale,
):
    sp_size = lax.axis_size("sp")
    tp_size = lax.axis_size("tp")
    rows_here = stream_in.shape[0]
    model_width = stream_in.shape[1]
    column_width = model_width // tp_size
    column_start = lax.axis_index("tp") * column_width
    capacity = 4 * rows_here // sp_size
    route_count = 2 * rows_here
    stream = stream_in.astype(jnp.float32)
    inverse_rms = lax.rsqrt(jnp.mean(stream * stream, axis=-1, keepdims=True) + norm_eps)
    unit_stream = stream * inverse_rms
    normed = (unit_stream * norm_gain).astype(jnp.bfloat16)
    slot_of_route, route_of_slot = slot_table(expert_choice, sp_size, capacity)
    present = route_of_slot < route_count
    safe_route = jnp.where(present, route_of_slot, 0)
    token = safe_route // 2
    weight = jnp.where(present, route_scale.reshape(-1)[safe_route], jnp.zeros((), jnp.float32))
    scaled_send = (cotangent[token].astype(jnp.float32) * weight[:, None]).astype(jnp.bfloat16)
    rows_send = jnp.where(present[:, None], normed[token], jnp.zeros((), jnp.bfloat16))
    scaled_part = lax.dynamic_slice_in_dim(scaled_send, column_start, column_width, 1)
    rows_part = lax.dynamic_slice_in_dim(rows_send, column_start, column_width, 1)
    scaled_recv, rows_recv = (
        lax.all_to_all(scaled_part, "sp", split_axis=0, concat_axis=0, tiled=True),
        lax.all_to_all(rows_part, "sp", split_axis=0, concat_axis=0, tiled=True),
    )
    scaled_cot, expert_rows = sent_together((scaled_recv, rows_recv), "tp", 1, 0)
    w_gate = expert_gate[0]
    w_up = expert_up[0]
    w_down = expert_down[0]
    gate_pre = jnp.dot(expert_rows, w_gate, preferred_element_type=jnp.float32)
    up_pre = jnp.dot(expert_rows, w_up, preferred_element_type=jnp.float32)
    sigmoid_gate = jax.nn.sigmoid(gate_pre)
    silu_gate = gate_pre * sigmoid_gate
    hidden = (silu_gate * up_pre).astype(jnp.bfloat16)
    hidden_grad = cols_product(scaled_cot, w_down)
    gate_grad = (
        hidden_grad * up_pre * sigmoid_gate * (1.0 + gate_pre * (1.0 - sigmoid_gate))
    ).astype(jnp.bfloat16)
    up_grad = (hidden_grad * silu_gate).astype(jnp.bfloat16)
    partial_grad = cols_product(gate_grad, w_gate) + cols_product(up_grad, w_up)
    slot_grad = sent_and_summed(partial_grad.astype(jnp.bfloat16), "tp", 1).astype(jnp.bfloat16)
    returned = lax.all_to_all(slot_grad, "sp", split_axis=0, concat_axis=0, tiled=True)
    grad_down = rows_product(hidden, scaled_cot)[None]
    grad_gate = rows_product(expert_rows, gate_grad)[None]
    grad_up = rows_product(expert_rows, up_grad)[None]
    product = in_gate.astype(jnp.float32) * conv_input.astype(jnp.float32)
    earlier = passed_along(product[-2:], "sp", 1)
    extended = jnp.concatenate([earlier, product], axis=0)
    filtered = conv_taps[0] * product + conv_taps[1] * extended[1:-1] + conv_taps[2] * extended[:-2]
    mixed_in = (out_gate.astype(jnp.float32) * filtered).astype(jnp.bfloat16)
    token_cols = returned[slot_of_route].astype(jnp.float32).reshape(rows_here, 2, column_width)
    token_cols = jnp.sum(token_cols, axis=1).astype(jnp.bfloat16)
    token_grad = gather_directly(token_cols, "tp", 1)
    unit_grad = token_grad.astype(jnp.float32) * norm_gain
    along = jnp.mean(unit_stream * unit_grad, axis=-1, keepdims=True)
    stream_grad = (
        cotangent.astype(jnp.float32) + inverse_rms * (unit_grad - unit_stream * along)
    ).astype(jnp.bfloat16)
    grad_stream = lax.dynamic_slice_in_dim(stream_grad, column_start, column_width, 1)
    mixed_grad = jnp.dot(stream_grad, out_weight, preferred_element_type=jnp.float32)
    grad_out_gate = (mixed_grad * filtered).astype(jnp.bfloat16)
    filtered_grad = mixed_grad * out_gate.astype(jnp.float32)
    later = passed_along(filtered_grad[:2], "sp", -1)
    extended_grad = jnp.concatenate([filtered_grad, later], axis=0)
    product_grad = (
        conv_taps[0] * filtered_grad
        + conv_taps[1] * extended_grad[1:-1]
        + conv_taps[2] * extended_grad[2:]
    )
    grad_in_gate = (product_grad * conv_input.astype(jnp.float32)).astype(jnp.bfloat16)
    grad_conv_input = (product_grad * in_gate.astype(jnp.float32)).astype(jnp.bfloat16)
    grad_out_weight = sent_and_summed(
        rows_product(stream_grad, mixed_in).astype(jnp.bfloat16), "sp", 0
    )
    return (
        grad_stream,
        grad_out_gate,
        grad_in_gate,
        grad_conv_input,
        grad_out_weight,
        grad_gate,
        grad_up,
        grad_down,
    )


def solution(mesh):
    placed = (
        P("sp", None),
        P("sp", None),
        P(),
        P("sp", "tp"),
        P("sp", "tp"),
        P("sp", "tp"),
        P(None, "tp"),
        P(None, "tp"),
        P("sp", None, "tp"),
        P("sp", None, "tp"),
        P("sp", "tp", None),
        P("sp", None),
        P("sp", None),
    )
    return jax.shard_map(
        shards,
        mesh=mesh,
        in_specs=placed,
        out_specs=(
            P("sp", "tp"),
            P("sp", "tp"),
            P("sp", "tp"),
            P("sp", "tp"),
            P("sp", "tp"),
            P("sp", None, "tp"),
            P("sp", None, "tp"),
            P("sp", "tp", None),
        ),
        check_vma=False,
    )
```

profile of v0, /device:TPU:1, one launch (start us, length us, event | category | flops | bytes accessed | tf_op | source)
XLA Modules:
  0.0 362.6 jit_solution(17873283977544928509)
XLA Ops:
  7.2 0.8 broadcast_multiply_fusion
  8.0 0.8 copy.27
  9.1 1.5 fusion.22
  10.9 1.2 reduce-window.6
  12.5 2.4 scatter_custom_fusion
  15.0 1.5 fusion.16
  16.6 6.0 %gather_fusion.2 = bf16[1024,2048]{1,0:T(8,128)(2,1)} fusion(bf16[256,2048]{1,0:T(8,128)(2,1)S(1)} %fusion.16, s32[1024]{0:T(1024)S(1)} %fusion.51), kind=kCustom, calls=%fused_computation.2 | custom fusion | bytes 8392704 | tf_op jit(solution)/shard_map/gather | solution.py:109
  22.6 2.6 dynamic-slice_select_fusion
  25.2 13.3 %all-to-all-start.1 = ((bf16[64,16,512]{2,1,0:T(8,128)(2,1)}), bf16[64,16,512]{2,1,0:T(8,128)(2,1)}, u32[]{:S(2)}, u32[]{:S(2)}) async-start(bf16[64,16,512]{2,1,0:T(8,128)(2,1)} %bitcast.5), calls=%async_computation.1 | async-start | bytes 2097152 | tf_op jit(solution)/shard_map/all_to_all | solution.py:114
  38.9 6.0 %gather_fusion = bf16[1024,2048]{1,0:T(8,128)(2,1)} fusion(bf16[256,2048]{1,0:T(8,128)(2,1)S(1)} %copy-done.2, s32[1024]{0:T(1024)S(1)} %fusion.51), kind=kCustom, calls=%fused_computation | custom fusion | bytes 8392704 | tf_op jit(solution)/shard_map/gather | solution.py:108
  44.9 6.9 %gather_fusion.1 = f32[1024]{0:T(1024)S(1)} fusion(f32[512]{0:T(512)S(1)} %reshape.98, s32[1024]{0:T(1024)S(1)} %get-tuple-element.12), kind=kCustom, calls=%fused_computation.1 | custom fusion | bytes 12288 | tf_op jit(solution)/shard_map/gather | solution.py:107
  51.8 1.5 multiply_convert_fusion
  53.3 13.3 %all-to-all-done.1 = bf16[64,16,512]{2,1,0:T(8,128)(2,1)} async-done(((bf16[64,16,512]{2,1,0:T(8,128)(2,1)}), bf16[64,16,512]{2,1,0:T(8,128)(2,1)}, u32[]{:S(2)}, u32[]{:S(2)}) %all-to-all-start.1) | async-done | bytes 1048608 | tf_op jit(solution)/shard_map/all_to_all | solution.py:114
  66.6 34.2 %all_to_all.51 = bf16[64,16,512]{2,1,0:T(8,128)(2,1)S(1)} all-to-all(bf16[64,16,512]{2,1,0:T(8,128)(2,1)S(1)} %bitcast.76), channel_id=1, replica_groups=mesh['sp'=64,'tp'=4] {'sp'}, dimensions={0} | all-to-all | bytes 2097152 | tf_op jit(solution)/shard_map/all_to_all | solution.py:113
  100.8 2.7 pad_maximum_fusion
  103.6 82.5 %all-gather.2.cloned.1.call-done = bf16[2048,2048]{1,0:T(8,128)(2,1)} async-done(((bf16[2048,512]{1,0:T(8,128)(2,1)}), bf16[2048,2048]{1,0:T(8,128)(2,1)}) %all-gather.2.cloned.1.call-update) | async-done | bytes 8388624 | tf_op jit(solution)/shard_map/all_gather | solution.py:12
  186.0 3.6 fusion.9
  189.6 1.0 copy-done.18
  190.7 1.3 fusion.11
  192.3 1.6 multiply_convert_fusion.2
  193.9 1.3 fusion.23
  195.2 1.3 add_convert_fusion
  196.5 0.4 copy.38
  196.9 51.3 %all_to_all.52 = bf16[4,1024,512]{2,1,0:T(8,128)(2,1)} all-to-all(bf16[4,1024,512]{2,1,0:T(8,128)(2,1)S(1)} %bitcast.75), channel_id=1, replica_groups=mesh['sp'=64,'tp'=4] {'tp'}, dimensions={0} | all-to-all | bytes 8388608 | tf_op jit(solution)/shard_map/all_to_all | solution.py:24
  248.3 4.1 %reduce_sum.65 = bf16[1024,512]{1,0:T(8,128)(2,1)} reduce(bf16[4,1024,512]{2,1,0:T(8,128)(2,1)} %all_to_all.52, bf16[]{:T(256)} %constant.48.clone.1), dimensions={0}, to_apply=%region_5.6 | reduce | flops 1572864 | bytes 5242882 | tf_op jit(solution)/shard_map/reduce_sum | solution.py:25
  252.4 12.0 %all-to-all-start.3 = ((bf16[64,16,512]{2,1,0:T(8,128)(2,1)}), bf16[64,16,512]{2,1,0:T(8,128)(2,1)S(1)}, u32[]{:S(2)}, u32[]{:S(2)}) async-start(bf16[64,16,512]{2,1,0:T(8,128)(2,1)} %bitcast.11), calls=%async_computation.3 | async-start | bytes 2097152 | tf_op jit(solution)/shard_map/all_to_all | solution.py:132
  264.4 28.2 %all-to-all-done.3 = bf16[64,16,512]{2,1,0:T(8,128)(2,1)S(1)} async-done(((bf16[64,16,512]{2,1,0:T(8,128)(2,1)}), bf16[64,16,512]{2,1,0:T(8,128)(2,1)S(1)}, u32[]{:S(2)}, u32[]{:S(2)}) %all-to-all-start.3) | async-done | bytes 1048608 | tf_op jit(solution)/shard_map/all_to_all | solution.py:132
  292.6 2.0 gather_fusion.3
  294.8 1.4 reduce_sum.66
  296.1 1.1 broadcast_in_dim.54
  297.2 3.5 all-to-all-start.4
  300.8 4.5 %collective-permute-start = (f32[2,256]{1,0:T(2,128)S(1)}, f32[2,256]{1,0:T(2,128)S(1)}, u32[]{:S(2)}, u32[]{:S(2)}) collective-permute-start(f32[2,256]{1,0:T(2,128)S(1)} %slice.56), channel_id=1, source_target_pairs={{0,4},{4,8},{8,12},{12,16},{16,20},{20,24},{24,28},{28,32},{32,36}... | collective-permute-start | bytes 6152 | tf_op jit(solution)/shard_map/ppermute | solution.py:31
  305.4 9.4 %all-to-all-done.4 = bf16[4,256,512]{2,1,0:T(8,128)(2,1)S(1)} async-done(((bf16[4,256,512]{2,1,0:T(8,128)(2,1)}), bf16[4,256,512]{2,1,0:T(8,128)(2,1)S(1)}, u32[]{:S(2)}, u32[]{:S(2)}) %all-to-all-start.4) | async-done | bytes 1048608 | tf_op jit(solution)/shard_map/all_to_all | solution.py:36
  315.3 0.5 fusion.17
  315.8 0.7 fusion.21
  316.6 1.2 multiply_convert_fusion.5
  317.8 1.5 convolution_convert_fusion
  319.4 7.4 %all-to-all-start.5 = ((bf16[64,32,256]{2,1,0:T(8,128)(2,1)}), bf16[64,32,256]{2,1,0:T(8,128)(2,1)S(1)}, u32[]{:S(2)}, u32[]{:S(2)}) async-start(bf16[64,32,256]{2,1,0:T(8,128)(2,1)} %bitcast.17), calls=%async_computation.5 | async-start | bytes 2097152 | tf_op jit(solution)/shard_map/all_to_all | solution.py:24
  326.8 5.0 %convolution_bitcast_fusion = f32[1,2048,256]{2,1,0:T(8,128)} fusion(bf16[1024,256]{1,0:T(8,128)(2,1)S(1)} %copy-done.8, bf16[2048,2048]{1,0:T(8,128)(2,1)} %all-gather.2.cloned.1.call-done), kind=kOutput, calls=%fused_computation.12 | convolution fusion | flops 1073741824 | bytes 6815744 | tf_op jit(solution)/shard_map/dot_general | solution.py:65
  331.8 5.0 %convolution_bitcast_fusion.1 = f32[1,2048,256]{2,1,0:T(8,128)} fusion(bf16[1024,256]{1,0:T(8,128)(2,1)S(1)} %copy-done.6, bf16[2048,2048]{1,0:T(8,128)(2,1)} %all-gather.2.cloned.1.call-done), kind=kOutput, calls=%fused_computation.13 | convolution fusion | flops 1073741824 | bytes 6815744 | tf_op jit(solution)/shard_map/dot_general | solution.py:65
  336.8 2.7 fusion.4
  339.5 2.4 collective-permute-start.1
  341.8 0.7 constant_dynamic-slice_fusion
  342.5 2.1 collective-permute-done.1
  344.7 0.8 fusion.38
  345.4 0.7 fusion.39
  346.1 8.8 %all-to-all-done.5 = bf16[64,32,256]{2,1,0:T(8,128)(2,1)S(1)} async-done(((bf16[64,32,256]{2,1,0:T(8,128)(2,1)}), bf16[64,32,256]{2,1,0:T(8,128)(2,1)S(1)}, u32[]{:S(2)}, u32[]{:S(2)}) %all-to-all-start.5) | async-done | bytes 1048608 | tf_op jit(solution)/shard_map/all_to_all | solution.py:24
  354.9 0.8 convert_reduce_fusion
  (83 shorter events, 2.5 us)
Async XLA Ops:
  7.2 178.9 %copy-start = (bf16[1,2048,256]{2,1,0:T(8,128)(2,1)S(1)}, bf16[1,2048,256]{2,1,0:T(8,128)(2,1)}, u32[]{:S(2)}) copy-start(bf16[1,2048,256]{2,1,0:T(8,128)(2,1)} %param.21) | copy-start | bytes 3145732
  22.6 16.0 %copy-start.17 = (f32[256,2]{0,1:T(2,128)S(1)}, f32[256,2]{0,1:T(2,128)}, u32[]{:S(2)}) copy-start(f32[256,2]{0,1:T(2,128)} %param.25) | copy-start | bytes 6148
  22.6 16.3 %copy-start.2 = (bf16[256,2048]{1,0:T(8,128)(2,1)S(1)}, bf16[256,2048]{1,0:T(8,128)(2,1)}, u32[]{:S(2)}) copy-start(bf16[256,2048]{1,0:T(8,128)(2,1)} %param.13) | copy-start | bytes 3145732
  25.2 41.4 %all-to-all-start.1 = ((bf16[64,16,512]{2,1,0:T(8,128)(2,1)}), bf16[64,16,512]{2,1,0:T(8,128)(2,1)}, u32[]{:S(2)}, u32[]{:S(2)}) async-start(bf16[64,16,512]{2,1,0:T(8,128)(2,1)} %bitcast.5), calls=%async_computation.1 | async-start | bytes 2097152 | tf_op jit(solution)/shard_map/all_to_all | solution.py:114
  38.5 147.5 %all-gather.2.cloned.1.call-start = ((), (), s32[]{:S(2)}) async-start(), calls=%async_computation.6 | async-start | bytes 10485760 | tf_op jit(solution)/shard_map/all_gather | solution.py:12
  103.5 86.1 %copy-start.4 = (bf16[1,2048,256]{2,1,0:T(8,128)(2,1)S(1)}, bf16[1,2048,256]{2,1,0:T(8,128)(2,1)}, u32[]{:S(2)}) copy-start(bf16[1,2048,256]{2,1,0:T(8,128)(2,1)} %param.22) | copy-start | bytes 3145732
  186.0 4.6 %copy-start.18 = (bf16[2048,2048]{1,0:T(8,128)(2,1)S(1)}, bf16[2048,2048]{1,0:T(8,128)(2,1)}, u32[]{:S(2)}) copy-start(bf16[2048,2048]{1,0:T(8,128)(2,1)} %all-gather.2.cloned.1.call-done) | copy-start | bytes 25165828
  190.7 1.3 copy-start.21
  190.7 1.6 copy-start.19
  192.3 1.6 copy-start.23
  193.9 1.3 copy-start.5
  193.9 1.3 copy-start.7
  252.4 40.2 %all-to-all-start.3 = ((bf16[64,16,512]{2,1,0:T(8,128)(2,1)}), bf16[64,16,512]{2,1,0:T(8,128)(2,1)S(1)}, u32[]{:S(2)}, u32[]{:S(2)}) async-start(bf16[64,16,512]{2,1,0:T(8,128)(2,1)} %bitcast.11), calls=%async_computation.3 | async-start | bytes 2097152 | tf_op jit(solution)/shard_map/all_to_all | solution.py:132
  292.6 8.2 %copy-start.9 = (bf16[256,256]{1,0:T(8,128)(2,1)S(1)}, bf16[256,256]{1,0:T(8,128)(2,1)}, u32[]{:S(2)}) copy-start(bf16[256,256]{1,0:T(8,128)(2,1)} %param.17) | copy-start | bytes 393220
  292.6 8.2 %copy-start.10 = (bf16[256,256]{1,0:T(8,128)(2,1)S(1)}, bf16[256,256]{1,0:T(8,128)(2,1)}, u32[]{:S(2)}) copy-start(bf16[256,256]{1,0:T(8,128)(2,1)} %param.18) | copy-start | bytes 393220
  292.6 12.8 %copy-start.16 = (f32[3,256]{1,0:T(4,128)S(1)}, f32[3,256]{1,0:T(4,128)}, u32[]{:S(2)}) copy-start(f32[3,256]{1,0:T(4,128)} %param.19) | copy-start | bytes 9220
  297.2 17.5 %all-to-all-start.4 = ((bf16[4,256,512]{2,1,0:T(8,128)(2,1)}), bf16[4,256,512]{2,1,0:T(8,128)(2,1)S(1)}, u32[]{:S(2)}, u32[]{:S(2)}) async-start(bf16[4,256,512]{2,1,0:T(8,128)(2,1)} %broadcast_in_dim.54), calls=%async_computation.4 | async-start | bytes 2097152 | tf_op jit(solution)/shard_map/all_to_all | solution.py:36
  300.7 14.5 %copy-start.3 = (bf16[256,2048]{1,0:T(8,128)(2,1)S(1)}, bf16[256,2048]{1,0:T(8,128)(2,1)}, u32[]{:S(2)}) copy-start(bf16[256,2048]{1,0:T(8,128)(2,1)} %param.14) | copy-start | bytes 3145732
  300.8 14.4 %copy-start.15 = (f32[2048]{0:T(1024)S(1)}, f32[2048]{0:T(1024)}, u32[]{:S(2)}) copy-start(f32[2048]{0:T(1024)} %param.15) | copy-start | bytes 24580
  300.8 4.5 %copy-start.12 = (f32[256,256]{1,0:T(8,128)}, f32[256,256]{1,0:T(8,128)S(1)}, u32[]{:S(2)}) copy-start(f32[256,256]{1,0:T(8,128)S(1)} %convert_multiply_fusion.5) | copy-start | bytes 786436
  300.8 15.7 %collective-permute-start = (f32[2,256]{1,0:T(2,128)S(1)}, f32[2,256]{1,0:T(2,128)S(1)}, u32[]{:S(2)}, u32[]{:S(2)}) collective-permute-start(f32[2,256]{1,0:T(2,128)S(1)} %slice.56), channel_id=1, source_target_pairs={{0,4},{4,8},{8,12},{12,16},{16,20},{20,24},{24,28},{28,32},{32,36}... | collective-permute-start | bytes 6152 | tf_op jit(solution)/shard_map/ppermute | solution.py:31
  315.2 1.3 copy-start.13
  315.2 1.3 copy-start.14
  315.2 1.4 copy-start.20
  316.5 10.2 %copy-start.8 = (bf16[1024,256]{1,0:T(8,128)(2,1)S(1)}, bf16[1024,256]{1,0:T(8,128)(2,1)}, u32[]{:S(2)}) copy-start(bf16[1024,256]{1,0:T(8,128)(2,1)} %copy-done.7) | copy-start | bytes 1572868
  319.4 35.6 %all-to-all-start.5 = ((bf16[64,32,256]{2,1,0:T(8,128)(2,1)}), bf16[64,32,256]{2,1,0:T(8,128)(2,1)S(1)}, u32[]{:S(2)}, u32[]{:S(2)}) async-start(bf16[64,32,256]{2,1,0:T(8,128)(2,1)} %bitcast.17), calls=%async_computation.5 | async-start | bytes 2097152 | tf_op jit(solution)/shard_map/all_to_all | solution.py:24
  326.8 5.0 %copy-start.6 = (bf16[1024,256]{1,0:T(8,128)(2,1)S(1)}, bf16[1024,256]{1,0:T(8,128)(2,1)}, u32[]{:S(2)}) copy-start(bf16[1024,256]{1,0:T(8,128)(2,1)} %copy-done.5) | copy-start | bytes 1572868
  326.8 10.0 %slice-start = ((s8[8388608]{0:T(1024)(128)(4,1)}), s8[4194304]{0:T(1024)(128)(4,1)S(1)}, s32[]{:S(2)}) async-start(s8[8388608]{0:T(1024)(128)(4,1)} %bitcast.87), calls=%async_computation.7 | async-start | bytes 8388608
  331.8 5.0 %slice-start.1 = ((s8[8388608]{0:T(1024)(128)(4,1)}), s8[4194304]{0:T(1024)(128)(4,1)S(1)}, s32[]{:S(2)}) async-start(s8[8388608]{0:T(1024)(128)(4,1)} %bitcast.87), calls=%async_computation.8 | async-start | bytes 8388608
  331.8 5.0 %copy-start.22 = (f32[1024,256]{1,0:T(8,128)S(1)}, f32[1024,256]{1,0:T(8,128)}, u32[]{:S(2)}) copy-start(f32[1024,256]{1,0:T(8,128)} %copy-done.21) | copy-start | bytes 3145732
  331.8 5.0 %copy-start.24 = (f32[1024,256]{1,0:T(8,128)S(1)}, f32[1024,256]{1,0:T(8,128)}, u32[]{:S(2)}) copy-start(f32[1024,256]{1,0:T(8,128)} %copy-done.23) | copy-start | bytes 3145732
  336.8 2.7 copy-start.11
  336.8 18.9 %copy-start.1 = (bf16[1,2048,256]{2,1,0:T(8,128)(2,1)S(1)}, bf16[1,2048,256]{2,1,0:T(8,128)(2,1)}, u32[]{:S(2)}) copy-start(bf16[1,2048,256]{2,1,0:T(8,128)(2,1)} %param.21) | copy-start | bytes 3145732
  339.5 5.2 %collective-permute-start.1 = (f32[2,256]{1,0:T(2,128)S(1)}, f32[2,256]{1,0:T(2,128)S(1)}, u32[]{:S(2)}, u32[]{:S(2)}) collective-permute-start(f32[2,256]{1,0:T(2,128)S(1)} %slice.59), channel_id=1, source_target_pairs={{4,0},{8,4},{12,8},{16,12},{20,16},{24,20},{28,24},{32,28},{36,32}... | collective-permute-start | bytes 6152 | tf_op jit(solution)/shard_map/ppermute | solution.py:31
Sparse Core Ops, SparseCore 0:
  103.7 82.3 all-gather.1
where the time goes:
time: 363 us
  waiting for transfers between devices  144 us (40%)
  blocking collectives  85.6 us (24%)
  starting transfers between devices  43.1 us (12%)
  local copies, waits for them, and re-layouts  29.3 us (8%)
  matrix products  24.4 us (7%)
  other arithmetic  21.4 us (6%)
  between operations  14.6 us (4%)
    all_gather x1, waiting for transfers between devices, sent_together(): filled = lax.all_gather(both, axis, axis=dim, tiled=True)  82.5 us
    all_to_all x1, blocking collectives, sent_and_summed(): lax.all_to_all(tiles, axis, split_axis=0, concat_axis=0, tiled=True)  51.3 us
    all_to_all x1, blocking collectives, shards(): lax.all_to_all(scaled_part, 'sp', split_axis=0, concat_axis=0, tiled=True)  34.2 us
    all_to_all x1, waiting for transfers between devices, shards(): lax.all_to_all(slot_grad, 'sp', split_axis=0, concat_axis=0, tiled=True)  28.2 us
    dot_general x4, matrix products, rows_product(): lax.dot_general(left, right, (((0,), (0,)), ((), ())), preferred_element_...  14.1 us
    all_to_all x1, starting transfers between devices, shards(): lax.all_to_all(rows_part, 'sp', split_axis=0, concat_axis=0, tiled=True)  13.3 us
    all_to_all x1, waiting for transfers between devices, shards(): lax.all_to_all(rows_part, 'sp', split_axis=0, concat_axis=0, tiled=True)  13.3 us
    all_to_all x1, starting transfers between devices, shards(): lax.all_to_all(slot_grad, 'sp', split_axis=0, concat_axis=0, tiled=True)  12 us
  transfers between devices with their start and end apart: 7, of which 6 were waited for; matrix products, arithmetic and copies ran while one was open for 9% of the time, Pallas kernels for 0%

commit v1 on v0

v1 whole, which is shorter than its diff:
```python
import functools

import jax
import jax.numpy as jnp
from jax import lax
from jax.experimental import pallas as pl
from jax.experimental.pallas import tpu as pltpu
from jax.sharding import PartitionSpec as P

norm_eps = 1e-06
MESH = pl.DeviceIdType.MESH
CAP = 16
BF = jnp.bfloat16
F32 = jnp.float32


def split_up(array, dim, peers):
    dims = array.shape
    tiles = array.reshape(*dims[:dim], peers, dims[dim] // peers, *dims[dim + 1 :])
    return jnp.moveaxis(tiles, dim, 0)


def sent_and_summed(array, axis, dim):
    tiles = split_up(array, dim, lax.axis_size(axis))
    arrived = lax.all_to_all(tiles, axis, split_axis=0, concat_axis=0, tiled=True)
    return arrived.astype(jnp.float32).sum(axis=0)


def passed_along(value, axis, steps):
    count = lax.axis_size(axis)
    first, last = (max(0, -steps), min(count, count - steps))
    return lax.ppermute(value, axis, [(source, source + steps) for source in range(first, last)])


def rows_product(left, right):
    return lax.dot_general(left, right, (((0,), (0,)), ((), ())), preferred_element_type=F32)


def cols_product(left, right):
    return lax.dot_general(left, right, (((1,), (1,)), ((), ())), preferred_element_type=F32)


def product_of(left, right):
    return jnp.dot(left, right, preferred_element_type=F32)


def loop(low, high, body):
    def step(i, carry):
        body(i)
        return carry

    lax.fori_loop(low, high, step, 0)


def offset_of(t):
    return lax.rem(t + lax.div(t + 7, 8), 8) + lax.div(t, 7)


def expert_kernel(
    plane, choice, scale, cot, stream, gain, wg, wu, wd,
    tok, out_gate, out_up, out_down,
    normed, pick, weight, send_all, send_part, rows, partial, summand, total, back, hidden, ggrad, ugrad,
    a_send, a_recv, right_send, left_send, from_left, from_right,
    fright_send, fleft_send, ffrom_left, ffrom_right,
    rs_send, rs_recv, ret_send, ret_recv, tok_send, tok_recv,
):
    me = lax.axis_index("sp")
    q = lax.axis_index("tp")
    right = lax.rem(q + 1, 4)
    left = lax.rem(q + 3, 4)
    z = lax.div(me, plane)
    place = lax.rem(me, plane)
    experts = 8 * plane
    span = plane * CAP
    tokens, width = cot.shape
    part = width // 4
    mine = pl.ds(pl.multiple_of(q * part, part), part)
    my_slots = pl.ds(pl.multiple_of(me * CAP, CAP), CAP)

    def span_of(plane_at):
        return pl.ds(pl.multiple_of(plane_at * span, span), span)

    def wait_for(ref, sem):
        pltpu.make_async_copy(ref, ref, sem).wait()

    barrier = pltpu.get_barrier_semaphore()

    def greet(k):
        pl.semaphore_signal(barrier, inc=1, device_id=(lax.rem(me + k, experts), q), device_id_type=MESH)

    loop(1, experts, greet)

    def greet_row(k):
        pl.semaphore_signal(barrier, inc=1, device_id=(me, lax.rem(q + k, 4)), device_id_type=MESH)

    loop(1, 4, greet_row)

    x = stream[...].astype(F32)
    inverse = lax.rsqrt(jnp.mean(x * x, axis=-1, keepdims=True) + norm_eps)
    normed[...] = ((x * inverse) * gain[...]).astype(BF)

    first, second = choice[0:1, :], choice[1:2, :]
    ids = lax.broadcasted_iota(jnp.int32, (experts, tokens), 0)
    is_first, is_second = ids == first, ids == second
    named = jnp.where(is_first | is_second, 1.0, 0.0).astype(BF)
    before = jnp.where(
        lax.broadcasted_iota(jnp.int32, (tokens, tokens), 0) < lax.broadcasted_iota(jnp.int32, (tokens, tokens), 1), 1.0, 0.0
    ).astype(BF)
    earlier = product_of(named, before)
    slot_first = first * CAP + jnp.sum(jnp.where(is_first, earlier, 0.0), axis=0, keepdims=True).astype(jnp.int32)
    slot_second = second * CAP + jnp.sum(jnp.where(is_second, earlier, 0.0), axis=0, keepdims=True).astype(jnp.int32)
    slots = lax.broadcasted_iota(jnp.int32, (experts * CAP, tokens), 0)
    at_first, at_second = slots == slot_first, slots == slot_second
    pick[...] = jnp.where(at_first | at_second, 1.0, 0.0).astype(BF)
    weight[...] = jnp.sum(
        jnp.where(at_first, scale[0:1, :], 0.0) + jnp.where(at_second, scale[1:2, :], 0.0), axis=1, keepdims=True
    )

    pl.semaphore_wait(barrier, experts + 2)

    def send_quarter(t):
        target = lax.rem(z + offset_of(t), 8)
        chosen = pick[span_of(target), :]
        send_part[t - 1, 0] = product_of(chosen, normed[:, mine]).astype(BF)
        send_part[t - 1, 1] = (product_of(chosen, cot[:, mine]) * weight[span_of(target), :]).astype(BF)

        def one(k):
            block = pl.ds(pl.multiple_of(k * CAP, CAP), CAP)
            pltpu.make_async_remote_copy(
                send_part.at[t - 1, :, block, :], rows.at[:, my_slots, mine], a_send.at[t], a_recv.at[t],
                device_id=(target * plane + k, q), device_id_type=MESH,
            ).start()

        loop(0, plane, one)

    loop(1, 6, send_quarter)

    def send_whole(i):
        t = i + 5 * lax.div(i + 1, 2)
        target = lax.rem(z + offset_of(t), 8)
        chosen = pick[span_of(target), :]
        send_all[i, 0] = product_of(chosen, normed[...]).astype(BF)
        send_all[i, 1] = (product_of(chosen, cot[...]) * weight[span_of(target), :]).astype(BF)

        def one(k):
            block = pl.ds(pl.multiple_of(k * CAP, CAP), CAP)

            @pl.when(target * plane + k != me)
            def _():
                pltpu.make_async_remote_copy(
                    send_all.at[i, :, block, :], rows.at[:, my_slots, :], a_send.at[t], a_recv.at[t],
                    device_id=(target * plane + k, q), device_id_type=MESH,
                ).start()

        loop(0, plane, one)

    loop(0, 3, send_whole)
    own = pl.ds(pl.multiple_of(place * CAP, CAP), CAP)
    rows[0, my_slots, :] = send_all[0, 0, own, :]
    rows[1, my_slots, :] = send_all[0, 1, own, :]

    def step(i):
        @pl.when((i >= 1) & (i < 6))
        def _():
            at = span_of(lax.rem(z + 8 - offset_of(i), 8))
            piece = rows.at[:, at, mine]
            wait_for(piece, a_recv.at[i])
            pltpu.make_async_remote_copy(
                piece, piece, right_send.at[i], from_left.at[i], device_id=(me, right), device_id_type=MESH
            ).start()
            pltpu.make_async_remote_copy(
                piece, piece, left_send.at[i], from_right.at[i], device_id=(me, left), device_id_type=MESH
            ).start()

        @pl.when((i >= 2) & (i < 7))
        def _():
            t = i - 1
            at = span_of(lax.rem(z + 8 - offset_of(t), 8))
            of_left = rows.at[:, at, pl.ds(pl.multiple_of(left * part, part), part)]
            of_right = rows.at[:, at, pl.ds(pl.multiple_of(right * part, part), part)]
            wait_for(of_left, from_left.at[t])
            half = rows.at[0, at, pl.ds(pl.multiple_of(left * part, part), part)]
            pltpu.make_async_remote_copy(
                half, half, fright_send.at[t], ffrom_left.at[t], device_id=(me, right), device_id_type=MESH
            ).start()
            wait_for(of_right, from_right.at[t])
            half = rows.at[1, at, pl.ds(pl.multiple_of(right * part, part), part)]
            pltpu.make_async_remote_copy(
                half, half, fleft_send.at[t], ffrom_right.at[t], device_id=(me, left), device_id_type=MESH
            ).start()

        @pl.when((i >= 2) & (i < 10))
        def _():
            t = i - 2
            at = span_of(lax.rem(z + 8 - offset_of(t), 8))

            @pl.when((t >= 1) & (t < 6))
            def _():
                far = pl.ds(pl.multiple_of(lax.rem(q + 2, 4) * part, part), part)
                wait_for(rows.at[0, at, far], ffrom_left.at[t])
                wait_for(rows.at[1, at, far], ffrom_right.at[t])

            @pl.when(t == 0)
            def _():
                others = rows.at[:, pl.ds(0, (plane - 1) * CAP), :]
                if plane > 1:
                    wait_for(others, a_recv.at[0])

            @pl.when(t >= 6)
            def _():
                wait_for(rows.at[:, at, :], a_recv.at[t])

            here = rows[0, at, :]
            gate_pre = product_of(here, wg[...])
            up_pre = product_of(here, wu[...])
            hidden_grad = cols_product(rows[1, at, :], wd[...])
            sigmoid_gate = jax.nn.sigmoid(gate_pre)
            silu_gate = gate_pre * sigmoid_gate
            hidden[at, :] = (silu_gate * up_pre).astype(BF)
            gate_grad = (hidden_grad * up_pre * sigmoid_gate * (1.0 + gate_pre * (1.0 - sigmoid_gate))).astype(BF)
            up_grad = (hidden_grad * silu_gate).astype(BF)
            ggrad[at, :] = gate_grad
            ugrad[at, :] = up_grad
            partial[at, :] = (cols_product(gate_grad, wg[...]) + cols_product(up_grad, wu[...])).astype(BF)

            def one(d):
                to = lax.rem(q + d, 4)
                pltpu.make_async_remote_copy(
                    partial.at[at, pl.ds(pl.multiple_of(to * part, part), part)], summand.at[d - 1, at, :],
                    rs_send.at[t], rs_recv.at[t], device_id=(me, to), device_id_type=MESH,
                ).start()

            loop(1, 4, one)

        @pl.when(i >= 4)
        def _():
            t = i - 4
            source = lax.rem(z + 8 - offset_of(t), 8)
            at = span_of(source)
            wait_for(summand.at[:, at, :], rs_recv.at[t])
            added = partial[at, mine].astype(F32)
            for d in range(3):
                added = added + summand[d, at, :].astype(F32)
            total[at, :] = added.astype(BF)

            def one(k):
                block = pl.ds(pl.multiple_of(source * span + k * CAP, CAP), CAP)

                @pl.when(source * plane + k != me)
                def _():
                    pltpu.make_async_remote_copy(
                        total.at[block, :], back.at[my_slots, :], ret_send, ret_recv,
                        device_id=(source * plane + k, q), device_id_type=MESH,
                    ).start()

            loop(0, plane, one)

    loop(0, 12, step)
    back[my_slots, :] = total[my_slots, :]

    chunk = min(256, width)

    def grads(m):
        cols = pl.ds(pl.multiple_of(m * chunk, chunk), chunk)
        here = rows[0, :, cols]
        out_gate[cols, :] = rows_product(here, ggrad[...])
        out_up[cols, :] = rows_product(here, ugrad[...])
        out_down[:, cols] = rows_product(hidden[...], rows[1, :, cols])

    loop(0, width // chunk, grads)

    wait_for(back.at[pl.ds(0, (experts - 1) * CAP), :], ret_recv)
    tok[:, mine] = rows_product(pick[...], back[...]).astype(BF)

    def share(d):
        pltpu.make_async_remote_copy(
            tok.at[:, mine], tok.at[:, mine], tok_send, tok_recv.at[d - 1],
            device_id=(me, lax.rem(q + d, 4)), device_id_type=MESH,
        ).start()

    loop(1, 4, share)

    def sent_rows(t):
        @pl.when((t >= 1) & (t < 6))
        def _():
            at = span_of(lax.rem(z + 8 - offset_of(t), 8))
            piece = rows.at[:, at, mine]
            wait_for(piece, a_send.at[t])
            wait_for(piece, right_send.at[t])
            wait_for(piece, left_send.at[t])
            wait_for(rows.at[0, at, mine], fright_send.at[t])
            wait_for(rows.at[0, at, mine], fleft_send.at[t])

        @pl.when(t == 0)
        def _():
            if plane > 1:
                wait_for(rows.at[:, pl.ds(0, (plane - 1) * CAP), :], a_send.at[0])

        @pl.when(t >= 6)
        def _():
            wait_for(rows.at[:, span_of(0), :], a_send.at[t])

        wait_for(summand.at[:, span_of(0), :], rs_send.at[t])

    loop(0, 8, sent_rows)
    wait_for(back.at[pl.ds(0, (experts - 1) * CAP), :], ret_send)

    def shared(d):
        wait_for(tok.at[:, mine], tok_recv.at[d])

    loop(0, 3, shared)
    wait_for(tok.at[:, pl.ds(0, 3 * part)], tok_send)


def through_experts(choice, scale, cot, stream, gain, wg, wu, wd, experts):
    tokens, width = cot.shape
    part = width // 4
    slots = experts * CAP
    plane = experts // 8
    hid = wg.shape[1]
    vm = pl.BlockSpec(memory_space=pltpu.VMEM)
    dma8 = pltpu.SemaphoreType.DMA((8,))
    return pl.pallas_call(
        functools.partial(expert_kernel, plane),
        name="experts",
        out_shape=(
            jax.ShapeDtypeStruct((tokens, width), BF),
            jax.ShapeDtypeStruct((width, hid), F32),
            jax.ShapeDtypeStruct((width, hid), F32),
            jax.ShapeDtypeStruct((hid, width), F32),
        ),
        in_specs=[vm] * 8,
        out_specs=(vm, vm, vm, vm),
        scratch_shapes=[
            pltpu.VMEM((tokens, width), BF),
            pltpu.VMEM((slots, tokens), BF),
            pltpu.VMEM((slots, 1), F32),
            pltpu.VMEM((3, 2, plane * CAP, width), BF),
            pltpu.VMEM((5, 2, plane * CAP, part), BF),
            pltpu.VMEM((2, slots, width), BF),
            pltpu.VMEM((slots, width), BF),
            pltpu.VMEM((3, slots, part), BF),
            pltpu.VMEM((slots, part), BF),
            pltpu.VMEM((slots, part), BF),
            pltpu.VMEM((slots, hid), BF),
            pltpu.VMEM((slots, hid), BF),
            pltpu.VMEM((slots, hid), BF),
        ]
        + [dma8] * 12
        + [
            pltpu.SemaphoreType.DMA,
            pltpu.SemaphoreType.DMA,
            pltpu.SemaphoreType.DMA,
            pltpu.SemaphoreType.DMA((3,)),
        ],
        compiler_params=pltpu.CompilerParams(
            collective_id=0, has_side_effects=True, vmem_limit_bytes=62 * 1024 * 1024
        ),
    )(choice, scale, cot, stream, gain, wg, wu, wd)


def shards(
    cotangent,
    stream_in,
    norm_gain,
    out_gate,
    in_gate,
    conv_input,
    conv_taps,
    out_weight,
    expert_gate,
    expert_up,
    expert_down,
    expert_choice,
    route_scale,
):
    sp_size = lax.axis_size("sp")
    tp_size = lax.axis_size("tp")
    model_width = stream_in.shape[1]
    column_width = model_width // tp_size
    column_start = lax.axis_index("tp") * column_width
    token_grad, grad_gate, grad_up, grad_down = through_experts(
        expert_choice.T, route_scale.T, cotangent, stream_in, norm_gain[None], expert_gate[0], expert_up[0], expert_down[0], sp_size
    )
    stream = stream_in.astype(F32)
    inverse_rms = lax.rsqrt(jnp.mean(stream * stream, axis=-1, keepdims=True) + norm_eps)
    unit_stream = stream * inverse_rms
    product = in_gate.astype(F32) * conv_input.astype(F32)
    earlier = passed_along(product[-2:], "sp", 1)
    extended = jnp.concatenate([earlier, product], axis=0)
    filtered = conv_taps[0] * product + conv_taps[1] * extended[1:-1] + conv_taps[2] * extended[:-2]
    mixed_in = (out_gate.astype(F32) * filtered).astype(BF)
    unit_grad = token_grad.astype(F32) * norm_gain
    along = jnp.mean(unit_stream * unit_grad, axis=-1, keepdims=True)
    stream_grad = (cotangent.astype(F32) + inverse_rms * (unit_grad - unit_stream * along)).astype(BF)
    grad_stream = lax.dynamic_slice_in_dim(stream_grad, column_start, column_width, 1)
    mixed_grad = jnp.dot(stream_grad, out_weight, preferred_element_type=F32)
    grad_out_gate = (mixed_grad * filtered).astype(BF)
    filtered_grad = mixed_grad * out_gate.astype(F32)
    later = passed_along(filtered_grad[:2], "sp", -1)
    extended_grad = jnp.concatenate([filtered_grad, later], axis=0)
    product_grad = (
        conv_taps[0] * filtered_grad
        + conv_taps[1] * extended_grad[1:-1]
        + conv_taps[2] * extended_grad[2:]
    )
    grad_in_gate = (product_grad * conv_input.astype(F32)).astype(BF)
    grad_conv_input = (product_grad * in_gate.astype(F32)).astype(BF)
    grad_out_weight = sent_and_summed(rows_product(stream_grad, mixed_in).astype(BF), "sp", 0)
    return (
        grad_stream,
        grad_out_gate,
        grad_in_gate,
        grad_conv_input,
        grad_out_weight,
        grad_gate[None],
        grad_up[None],
        grad_down[None],
    )


def solution(mesh):
    placed = (
        P("sp", None),
        P("sp", None),
        P(),
        P("sp", "tp"),
        P("sp", "tp"),
        P("sp", "tp"),
        P(None, "tp"),
        P(None, "tp"),
        P("sp", None, "tp"),
        P("sp", None, "tp"),
        P("sp", "tp", None),
        P("sp", None),
        P("sp", None),
    )
    return jax.shard_map(
        shards,
        mesh=mesh,
        in_specs=placed,
        out_specs=(
            P("sp", "tp"),
            P("sp", "tp"),
            P("sp", "tp"),
            P("sp", "tp"),
            P("sp", "tp"),
            P("sp", None, "tp"),
            P("sp", None, "tp"),
            P("sp", "tp", None),
        ),
        check_vma=False,
    )
```

time: 363 us -> 222 us (0.61)
  Pallas kernels: 0 us -> 155 us
  waiting for transfers between devices: 144 us -> 21.6 us
  blocking collectives: 85.6 us -> 0 us
  matrix products: 24.4 us -> 2.65 us
  local copies, waits for them, and re-layouts: 29.3 us -> 8.35 us
  starting transfers between devices: 43.1 us -> 22.7 us
  between operations: 14.6 us -> 0.81 us
  other arithmetic: 21.4 us -> 10.5 us
    pallas_call x0 -> x1, Pallas kernels: none -> 155 us  [through_experts(): pl.pallas_call(functools.partial(expert_kernel, plane), name='experts', o...]
    all_to_all x2 -> x0, blocking collectives: 85.6 us -> none  [the longest x1 51.3 us: sent_and_summed(): lax.all_to_all(tiles, axis, split_axis=0, concat_axis=0, tiled=True)]
    all_gather x1 -> x0, waiting for transfers between devices: 82.5 us -> none  [sent_together(): filled = lax.all_gather(both, axis, axis=dim, tiled=True)]
    all_to_all x3 -> x0, waiting for transfers between devices: 50.8 us -> none  [the longest x1 28.2 us: shards(): lax.all_to_all(slot_grad, 'sp', split_axis=0, concat_axis=0, tiled=True)]
    all_to_all x3 -> x0, starting transfers between devices: 28.9 us -> none  [the longest x1 13.3 us: shards(): lax.all_to_all(rows_part, 'sp', split_axis=0, concat_axis=0, tiled=True)]
    gather x5 -> x0, local copies, waits for them, and re-layouts: 21.1 us -> none  [the longest x1 6.86 us: shards(): route_scale.reshape(-1)[safe_route]]
    dot_general x4 -> x1, matrix products: 14.1 us -> 1.47 us  [rows_product(): lax.dot_general(left, right, (((0,), (0,)), ((), ())), preferred_element_...]
    all_to_all x1, waiting for transfers between devices: 8.81 us -> 19.5 us  [sent_and_summed(): lax.all_to_all(tiles, axis, split_axis=0, concat_axis=0, tiled=True)]
  transfers between devices with their start and end apart: 7 -> 3, of which waited for: 6 -> 2; matrix products, arithmetic and copies ran while one was open for 9% -> 5% of each run, Pallas kernels for 0% -> 70%
where the time goes in v1:
time: 222 us; the launch traced here: 221 us
  Pallas kernels  155 us (70%)
  starting transfers between devices  22.7 us (10%)
  waiting for transfers between devices  21.6 us (10%)
  other arithmetic  10.5 us (5%)
  local copies, waits for them, and re-layouts  8.35 us (4%)
  matrix products  2.65 us (1%)
    pallas_call x1, Pallas kernels, through_experts(): pl.pallas_call(functools.partial(expert_kernel, plane), name='experts', o...  155 us
    all_to_all x1, waiting for transfers between devices, sent_and_summed(): lax.all_to_all(tiles, axis, split_axis=0, concat_axis=0, tiled=True)  19.5 us
    all_to_all x1, starting transfers between devices, sent_and_summed(): lax.all_to_all(tiles, axis, split_axis=0, concat_axis=0, tiled=True)  15.8 us
    ppermute x2, starting transfers between devices, passed_along(): lax.ppermute(value, axis, [(source, source + steps) for source in range(f...  6.93 us
    unnamed x23, local copies, waits for them, and re-layouts  6.91 us
  transfers between devices with their start and end apart: 3, of which 2 were waited for; matrix products, arithmetic and copies ran while one was open for 5% of the time, Pallas kernels for 70%

profile of v1, /device:TPU:1, one launch (start us, length us, event | category | flops | bytes accessed | tf_op | source)
XLA Modules:
  0.0 221.4 jit_solution(14378887917251555152)
XLA Ops:
  0.6 0.0 copy-start
  0.6 1.1 convert_multiply_fusion.6
  1.7 4.6 %collective-permute-start = (f32[2,256]{1,0:T(2,128)S(1)}, f32[2,256]{1,0:T(2,128)S(1)}, u32[]{:S(2)}, u32[]{:S(2)}) collective-permute-start(f32[2,256]{1,0:T(2,128)S(1)} %slice.39), channel_id=1, source_target_pairs={{0,4},{4,8},{8,12},{12,16},{16,20},{20,24},{24,28},{28,32},{32,36}... | collective-permute-start | bytes 6152 | tf_op jit(solution)/shard_map/ppermute | solution.py:32
  6.3 1.5 fusion.7
  7.9 0.0 copy-start.8
  7.9 154.9 %experts.1 = (bf16[256,2048]{1,0:T(8,128)(2,1)}, f32[2048,256]{1,0:T(8,128)}, f32[2048,256]{1,0:T(8,128)}, f32[256,2048]{1,0:T(8,128)}) custom-call(s32[2,256]{1,0:T(2,128)} %bitcast.30, f32[2,256]{1,0:T(2,128)} %bitcast.31, bf16[256,2048]{1,0:T(8,128)(2,1)} %cot.1, bf16[256,2048]{1,0:T(8,128)(2,1)} %stream.1, f32[1,2048]{1,0:T(1,128)} %bitcast.23, ...), custom_call_target="tpu_custom_call" | custom-call | tf_op jit(solution)/shard_map/experts/pallas_call | solution.py:323
  162.7 0.0 copy-start.1
  162.8 0.0 copy-start.2
  162.8 0.0 copy-done.8
  162.8 2.2 %fusion.2 = f32[256]{0:T(256)S(1)} fusion(bf16[256,2048]{1,0:T(8,128)(2,1)} %stream.1, bf16[256,2048]{1,0:T(8,128)(2,1)} %get-tuple-element.12, f32[2048]{0:T(1024)S(1)} %copy-done.8, f32[256]{0:T(256)S(1)} %add_rsqrt_fusion), kind=kLoop, calls=%fused_computation.5 | loop fusion | flops 3145472 | bytes 2107392 | tf_op jit(solution)/shard_map/reduce_sum | solution.py:394
  165.0 0.0 copy-done.1
  165.0 0.0 copy-done.2
  165.0 0.0 copy-start.9
  165.0 0.0 copy-start.7
  165.1 2.1 fusion.6
  167.1 0.0 copy-done.9
  167.2 0.0 collective-permute-done
  167.2 0.0 copy-done
  167.2 0.0 copy-done.7
  167.2 1.2 multiply_convert_fusion
  168.4 0.0 copy-start.5
  168.4 1.5 convolution_convert_fusion
  169.8 0.0 copy-start.6
  169.8 15.8 %all-to-all-start = ((bf16[64,32,256]{2,1,0:T(8,128)(2,1)}), bf16[64,32,256]{2,1,0:T(8,128)(2,1)S(1)}, u32[]{:S(2)}, u32[]{:S(2)}) async-start(bf16[64,32,256]{2,1,0:T(8,128)(2,1)} %bitcast.16), calls=%async_computation | async-start | bytes 2097152 | tf_op jit(solution)/shard_map/all_to_all | solution.py:25
  185.6 0.7 slice.42
  186.3 2.4 %collective-permute-start.1 = (f32[2,256]{1,0:T(2,128)S(1)}, f32[2,256]{1,0:T(2,128)S(1)}, u32[]{:S(2)}, u32[]{:S(2)}) collective-permute-start(f32[2,256]{1,0:T(2,128)S(1)} %slice.42), channel_id=1, source_target_pairs={{4,0},{8,4},{12,8},{16,12},{20,16},{24,20},{28,24},{32,28},{36,32}... | collective-permute-start | bytes 6152 | tf_op jit(solution)/shard_map/ppermute | solution.py:32
  188.7 0.7 constant_dynamic-slice_fusion
  189.4 2.1 collective-permute-done.1
  191.5 0.0 copy-done.5
  191.5 2.1 fusion.16
  193.6 0.0 copy-done.6
  193.6 0.7 fusion.17
  194.3 19.5 %all-to-all-done = bf16[64,32,256]{2,1,0:T(8,128)(2,1)S(1)} async-done(((bf16[64,32,256]{2,1,0:T(8,128)(2,1)}), bf16[64,32,256]{2,1,0:T(8,128)(2,1)S(1)}, u32[]{:S(2)}, u32[]{:S(2)}) %all-to-all-start) | async-done | bytes 1048608 | tf_op jit(solution)/shard_map/all_to_all | solution.py:25
  213.8 0.8 convert_reduce_fusion
  214.6 0.0 copy-start.4
  214.6 3.2 %copy.24 = f32[1,2048,256]{2,1,0:T(8,128)} copy(f32[1,2048,256]{2,1,0:T(8,128)} %bitcast.19) | data formatting | bytes 4194304
  217.8 0.0 copy-done.4
  217.8 0.0 copy-start.3
  217.8 1.3 copy.25
  219.1 1.0 copy-done.3
  220.1 1.3 copy.26
  (4 shorter events, 0.0 us)
Async XLA Ops:
  0.6 166.5 %copy-start = (bf16[2048,256]{1,0:T(8,128)(2,1)S(1)}, bf16[2048,256]{1,0:T(8,128)(2,1)}, u32[]{:S(2)}) copy-start(bf16[2048,256]{1,0:T(8,128)(2,1)} %param.20) | copy-start | bytes 3145732
  1.7 165.4 %collective-permute-start = (f32[2,256]{1,0:T(2,128)S(1)}, f32[2,256]{1,0:T(2,128)S(1)}, u32[]{:S(2)}, u32[]{:S(2)}) collective-permute-start(f32[2,256]{1,0:T(2,128)S(1)} %slice.39), channel_id=1, source_target_pairs={{0,4},{4,8},{8,12},{12,16},{16,20},{20,24},{24,28},{28,32},{32,36}... | collective-permute-start | bytes 6152 | tf_op jit(solution)/shard_map/ppermute | solution.py:32
  7.9 154.9 %copy-start.8 = (f32[2048]{0:T(1024)S(1)}, f32[2048]{0:T(1024)}, u32[]{:S(2)}) copy-start(f32[2048]{0:T(1024)} %param.15) | copy-start | bytes 24580
  162.7 2.3 %copy-start.1 = (bf16[256,2048]{1,0:T(8,128)(2,1)S(1)}, bf16[256,2048]{1,0:T(8,128)(2,1)}, u32[]{:S(2)}) copy-start(bf16[256,2048]{1,0:T(8,128)(2,1)} %stream.1) | copy-start | bytes 3145732
  162.8 2.3 %copy-start.2 = (bf16[256,2048]{1,0:T(8,128)(2,1)S(1)}, bf16[256,2048]{1,0:T(8,128)(2,1)}, u32[]{:S(2)}) copy-start(bf16[256,2048]{1,0:T(8,128)(2,1)} %get-tuple-element.12) | copy-start | bytes 3145732
  165.0 2.1 copy-start.9
  165.0 2.1 copy-start.7
  168.4 23.2 %copy-start.5 = (bf16[256,256]{1,0:T(8,128)(2,1)S(1)}, bf16[256,256]{1,0:T(8,128)(2,1)}, u32[]{:S(2)}) copy-start(bf16[256,256]{1,0:T(8,128)(2,1)} %param.17) | copy-start | bytes 393220
  169.8 23.8 %copy-start.6 = (bf16[256,256]{1,0:T(8,128)(2,1)S(1)}, bf16[256,256]{1,0:T(8,128)(2,1)}, u32[]{:S(2)}) copy-start(bf16[256,256]{1,0:T(8,128)(2,1)} %param.18) | copy-start | bytes 393220
  169.8 43.9 %all-to-all-start = ((bf16[64,32,256]{2,1,0:T(8,128)(2,1)}), bf16[64,32,256]{2,1,0:T(8,128)(2,1)S(1)}, u32[]{:S(2)}, u32[]{:S(2)}) async-start(bf16[64,32,256]{2,1,0:T(8,128)(2,1)} %bitcast.16), calls=%async_computation | async-start | bytes 2097152 | tf_op jit(solution)/shard_map/all_to_all | solution.py:25
  186.3 5.2 %collective-permute-start.1 = (f32[2,256]{1,0:T(2,128)S(1)}, f32[2,256]{1,0:T(2,128)S(1)}, u32[]{:S(2)}, u32[]{:S(2)}) collective-permute-start(f32[2,256]{1,0:T(2,128)S(1)} %slice.42), channel_id=1, source_target_pairs={{4,0},{8,4},{12,8},{16,12},{20,16},{24,20},{28,24},{32,28},{36,32}... | collective-permute-start | bytes 6152 | tf_op jit(solution)/shard_map/ppermute | solution.py:32
  214.6 3.2 %copy-start.4 = (f32[2048,256]{1,0:T(8,128)S(1)}, f32[2048,256]{1,0:T(8,128)}, u32[]{:S(2)}) copy-start(f32[2048,256]{1,0:T(8,128)} %get-tuple-element.14) | copy-start | bytes 6291460
  217.8 2.3 %copy-start.3 = (f32[256,2048]{1,0:T(8,128)S(1)}, f32[256,2048]{1,0:T(8,128)}, u32[]{:S(2)}) copy-start(f32[256,2048]{1,0:T(8,128)} %get-tuple-element.15) | copy-start | bytes 6291460

commit v2 on v1

v2 whole, which is shorter than its diff:
```python
import functools

import jax
import jax.numpy as jnp
from jax import lax
from jax.experimental import pallas as pl
from jax.experimental.pallas import tpu as pltpu
from jax.sharding import PartitionSpec as P

norm_eps = 1e-06
MESH = pl.DeviceIdType.MESH
CAP = 16
BF = jnp.bfloat16
F32 = jnp.float32


def rows_product(left, right):
    return lax.dot_general(left, right, (((0,), (0,)), ((), ())), preferred_element_type=F32)


def cols_product(left, right):
    return lax.dot_general(left, right, (((1,), (1,)), ((), ())), preferred_element_type=F32)


def product_of(left, right):
    return jnp.dot(left, right, preferred_element_type=F32)


def loop(low, high, body):
    def step(i, carry):
        body(i)
        return carry

    lax.fori_loop(low, high, step, 0)


def offset_of(t):
    half = lax.div(t + 1, 2)
    odd = lax.rem(t, 2)
    spread = odd * (1 + half) + (1 - odd) * (7 - half)
    return spread + 7 * lax.div(t + 7, 8) - 7 + 3 * lax.div(t, 6) - 7 * lax.div(t, 7)


def rows_at(index, count):
    return pl.ds(pl.multiple_of(index * count, count), count)


def step_kernel(
    plane, choice, scale, cot, stream, gain, og, ig, ci, taps, wg_hbm, wu_hbm, wd_hbm, ow_hbm,
    out_stream, out_og, out_ig, out_ci, out_ow, out_gate, out_up, out_down,
    wg, wu, wd, ow, inverse, normed, pick, weight, send_all, send_part, rows, partial, summand, total, back,
    hidden, ggrad, ugrad, gate_out, up_out, down_out, tok, sgrad, extended, filtered, mixed, fgrad,
    owp, pair, psum, arrived,
    in_sem, out_sem,
    a_send, a_recv, right_send, left_send, from_left, from_right,
    fright_send, fleft_send, ffrom_left, ffrom_right,
    rs_send, rs_recv, tright_send, tleft_send, tfrom_left, tfrom_right, tf_send, tf_recv, one_send, one_recv,
):
    me = lax.axis_index("sp")
    q = lax.axis_index("tp")
    right = lax.rem(q + 1, 4)
    left = lax.rem(q + 3, 4)
    z = lax.div(me, plane)
    place = lax.rem(me, plane)
    experts = 8 * plane
    span = plane * CAP
    tokens, width = cot.shape
    part = width // 4
    mine = rows_at(q, part)
    of_left = rows_at(left, part)
    of_right = rows_at(right, part)
    of_far = rows_at(lax.rem(q + 2, 4), part)
    my_slots = rows_at(me, CAP)

    def copy_to(src, dst, send, recv, sp, tp):
        pltpu.make_async_remote_copy(src, dst, send, recv, device_id=(sp, tp), device_id_type=MESH).start()

    def wait_for(ref, sem):
        pltpu.make_async_copy(ref, ref, sem).wait()

    def source_at(t):
        return lax.rem(z + 8 - offset_of(t), 8)

    def next_place(k):
        return lax.rem(place + k, plane)

    weights = (
        pltpu.make_async_copy(wg_hbm, wg, in_sem.at[0]),
        pltpu.make_async_copy(wu_hbm, wu, in_sem.at[1]),
        pltpu.make_async_copy(wd_hbm, wd, in_sem.at[2]),
        pltpu.make_async_copy(ow_hbm, ow, in_sem.at[3]),
    )
    for copy in weights:
        copy.start()

    barrier = pltpu.get_barrier_semaphore()

    def greet(k):
        pl.semaphore_signal(barrier, inc=1, device_id=(lax.rem(me + k, experts), q), device_id_type=MESH)

    loop(1, experts, greet)

    def greet_row(k):
        pl.semaphore_signal(barrier, inc=1, device_id=(me, lax.rem(q + k, 4)), device_id_type=MESH)

    loop(1, 4, greet_row)

    def norm_rows(r):
        at = rows_at(r, 16)
        x = stream[at, :].astype(F32)
        inv = lax.rsqrt(jnp.mean(x * x, axis=-1, keepdims=True) + norm_eps)
        inverse[at, :] = inv
        normed[at, :] = ((x * inv) * gain[...]).astype(BF)

    loop(0, tokens // 16, norm_rows)

    first, second = choice[0:1, :], choice[1:2, :]
    ids = lax.broadcasted_iota(jnp.int32, (experts, tokens), 0)
    is_first, is_second = ids == first, ids == second
    named = jnp.where(is_first | is_second, 1.0, 0.0).astype(BF)
    before = jnp.where(
        lax.broadcasted_iota(jnp.int32, (tokens, tokens), 0) < lax.broadcasted_iota(jnp.int32, (tokens, tokens), 1), 1.0, 0.0
    ).astype(BF)
    earlier = product_of(named, before)
    slot_first = first * CAP + jnp.sum(jnp.where(is_first, earlier, 0.0), axis=0, keepdims=True).astype(jnp.int32)
    slot_second = second * CAP + jnp.sum(jnp.where(is_second, earlier, 0.0), axis=0, keepdims=True).astype(jnp.int32)

    def pick_rows(p):
        slots = lax.broadcasted_iota(jnp.int32, (span, tokens), 0) + p * span
        at_first, at_second = slots == slot_first, slots == slot_second
        pick[rows_at(p, span), :] = jnp.where(at_first | at_second, 1.0, 0.0).astype(BF)
        weight[rows_at(p, span), :] = jnp.sum(
            jnp.where(at_first, scale[0:1, :], 0.0) + jnp.where(at_second, scale[1:2, :], 0.0), axis=1, keepdims=True
        )

    loop(0, 8, pick_rows)

    def fill_quarter(t):
        at = rows_at(lax.rem(z + offset_of(t), 8), span)
        chosen = pick[at, :]
        send_part[t - 1, 0] = product_of(chosen, normed[:, mine]).astype(BF)
        send_part[t - 1, 1] = (product_of(chosen, cot[:, mine]) * weight[at, :]).astype(BF)

    loop(1, 6, fill_quarter)

    def turn_of(i):
        return i + 5 * lax.div(i + 1, 2)

    def fill_whole(i):
        at = rows_at(lax.rem(z + offset_of(turn_of(i)), 8), span)
        chosen = pick[at, :]
        send_all[i, 0] = product_of(chosen, normed[...]).astype(BF)
        send_all[i, 1] = (product_of(chosen, cot[...]) * weight[at, :]).astype(BF)

    loop(0, 3, fill_whole)
    own = rows_at(place, CAP)
    rows[0, my_slots, :] = send_all[0, 0, own, :]
    rows[1, my_slots, :] = send_all[0, 1, own, :]

    extended[8 : tokens + 8, :] = ig[...].astype(F32) * ci[...].astype(F32)

    @pl.when(me == 0)
    def _():
        extended[0:8, :] = jnp.zeros((8, part_of(extended)), F32)

    pl.semaphore_wait(barrier, experts + 2)

    @pl.when(me < experts - 1)
    def _():
        copy_to(extended.at[tokens : tokens + 8], extended.at[0:8], one_send.at[0], one_recv.at[0], me + 1, q)

    def send_quarter(t):
        target = lax.rem(z + offset_of(t), 8)

        def one(k):
            to = next_place(k)
            copy_to(
                send_part.at[t - 1, :, rows_at(to, CAP), :], rows.at[:, my_slots, mine],
                a_send.at[t], a_recv.at[t], target * plane + to, q,
            )

        loop(0, plane, one)

    loop(1, 6, send_quarter)

    def send_whole(i):
        t = turn_of(i)
        target = lax.rem(z + offset_of(t), 8)

        def one(k):
            to = next_place(k)

            @pl.when(target * plane + to != me)
            def _():
                copy_to(
                    send_all.at[i, :, rows_at(to, CAP), :], rows.at[:, my_slots, :],
                    a_send.at[t], a_recv.at[t], target * plane + to, q,
                )

        loop(0, plane, one)

    loop(0, 3, send_whole)

    @pl.when(me > 0)
    def _():
        wait_for(extended.at[0:8], one_recv.at[0])

    now = (
        taps[0:1, :] * extended[8 : tokens + 8, :]
        + taps[1:2, :] * extended[7 : tokens + 7, :]
        + taps[2:3, :] * extended[6 : tokens + 6, :]
    )
    filtered[...] = now
    mixed[...] = (og[...].astype(F32) * now).astype(BF)
    for copy in weights:
        copy.wait()

    def step(i):
        @pl.when((i >= 1) & (i < 6))
        def _():
            piece = rows.at[:, rows_at(source_at(i), span), mine]
            wait_for(piece, a_recv.at[i])
            copy_to(piece, piece, right_send.at[i], from_left.at[i], me, right)
            copy_to(piece, piece, left_send.at[i], from_right.at[i], me, left)

        @pl.when((i >= 2) & (i < 7))
        def _():
            t = i - 1
            at = rows_at(source_at(t), span)
            wait_for(rows.at[:, at, of_left], from_left.at[t])
            half = rows.at[0, at, of_left]
            copy_to(half, half, fright_send.at[t], ffrom_left.at[t], me, right)
            wait_for(rows.at[:, at, of_right], from_right.at[t])
            half = rows.at[1, at, of_right]
            copy_to(half, half, fleft_send.at[t], ffrom_right.at[t], me, left)

        @pl.when((i == 0) | ((i >= 3) & (i < 10)))
        def _():
            t = (i - 2) * lax.div(i + 13, 16)
            at = rows_at(source_at(t), span)

            @pl.when((t >= 1) & (t < 6))
            def _():
                wait_for(rows.at[0, at, of_far], ffrom_left.at[t])
                wait_for(rows.at[1, at, of_far], ffrom_right.at[t])

            @pl.when(t == 0)
            def _():
                if plane > 1:
                    wait_for(rows.at[:, pl.ds(0, (plane - 1) * CAP), :], a_recv.at[0])

            @pl.when(t >= 6)
            def _():
                wait_for(rows.at[:, at, :], a_recv.at[t])

            here = rows[0, at, :]
            gate_pre = product_of(here, wg[...])
            up_pre = product_of(here, wu[...])
            hidden_grad = cols_product(rows[1, at, :], wd[...])
            sigmoid_gate = jax.nn.sigmoid(gate_pre)
            silu_gate = gate_pre * sigmoid_gate
            hidden[at, :] = (silu_gate * up_pre).astype(BF)
            gate_grad = (hidden_grad * up_pre * sigmoid_gate * (1.0 + gate_pre * (1.0 - sigmoid_gate))).astype(BF)
            up_grad = (hidden_grad * silu_gate).astype(BF)
            ggrad[at, :] = gate_grad
            ugrad[at, :] = up_grad
            partial[at, :] = (cols_product(gate_grad, wg[...]) + cols_product(up_grad, wu[...])).astype(BF)

            def one(d):
                to = lax.rem(q + d, 4)
                copy_to(partial.at[at, rows_at(to, part)], summand.at[d - 1, at, :], rs_send.at[t], rs_recv.at[t], me, to)

            loop(1, 4, one)

        @pl.when(i >= 3)
        def _():
            t = i - 3
            source = source_at(t)
            at = rows_at(source, span)
            wait_for(summand.at[:, at, :], rs_recv.at[t])
            added = partial[at, mine].astype(F32)
            for d in range(3):
                added = added + summand[d, at, :].astype(F32)
            total[at, :] = added.astype(BF)

            def one(k):
                to = source * plane + next_place(k)

                @pl.when(to != me)
                def _():
                    copy_to(total.at[rows_at(to, CAP), :], back.at[my_slots, :], one_send.at[1], one_recv.at[1], to, q)

            loop(0, plane, one)

    loop(0, 11, step)
    back[my_slots, :] = total[my_slots, :]

    chunk = min(256, width)

    def grads(m):
        cols = rows_at(m, chunk)
        here = rows[0, :, cols]
        gate_out[cols, :] = rows_product(here, ggrad[...]).astype(BF)
        up_out[cols, :] = rows_product(here, ugrad[...]).astype(BF)
        down_out[:, cols] = rows_product(hidden[...], rows[1, :, cols]).astype(BF)

    loop(0, width // chunk, grads)
    finished = (
        pltpu.make_async_copy(gate_out, out_gate, out_sem.at[0]),
        pltpu.make_async_copy(up_out, out_up, out_sem.at[1]),
        pltpu.make_async_copy(down_out, out_down, out_sem.at[2]),
    )
    for copy in finished:
        copy.start()

    wait_for(back.at[pl.ds(0, (experts - 1) * CAP), :], one_recv.at[1])
    tok[:, mine] = rows_product(pick[...], back[...]).astype(BF)
    half = tokens // 2
    low, high = pl.ds(0, half), pl.ds(half, half)
    for h, at in ((0, low), (1, high)):
        copy_to(tok.at[at, mine], tok.at[at, mine], tright_send.at[h], tfrom_left.at[h], me, right)
    for h, at in ((1, high), (0, low)):
        copy_to(tok.at[at, mine], tok.at[at, mine], tleft_send.at[h], tfrom_right.at[h], me, left)
    wait_for(tok.at[low, of_left], tfrom_left.at[0])
    copy_to(tok.at[low, of_left], tok.at[low, of_left], tf_send.at[0], tf_recv.at[0], me, right)
    wait_for(tok.at[high, of_right], tfrom_right.at[1])
    copy_to(tok.at[high, of_right], tok.at[high, of_right], tf_send.at[1], tf_recv.at[1], me, left)
    wait_for(tok.at[high, of_left], tfrom_left.at[1])
    wait_for(tok.at[low, of_right], tfrom_right.at[0])
    wait_for(tok.at[low, of_far], tf_recv.at[0])
    wait_for(tok.at[high, of_far], tf_recv.at[1])

    def stream_rows(r):
        at = rows_at(r, 16)
        inv = inverse[at, :]
        unit = stream[at, :].astype(F32) * inv
        unit_grad = tok[at, :].astype(F32) * gain[...]
        along = jnp.mean(unit * unit_grad, axis=-1, keepdims=True)
        sgrad[at, :] = (cot[at, :].astype(F32) + inv * (unit_grad - unit * along)).astype(BF)

    loop(0, tokens // 16, stream_rows)

    block = width // experts
    pairs = experts // 2
    core = lax.rem(me, 2)
    here = lax.div(me, 2)
    chunks = min(8, pairs)
    groups = pairs // chunks
    cut = 2 * groups * block

    def out_rows(m):
        found = rows_product(sgrad[:, rows_at(m, cut)], mixed[...]).astype(BF)
        owp[rows_at(m, groups)] = found.reshape(groups, 2, block, found.shape[-1])

    loop(0, chunks, out_rows)
    copy_to(owp.at[:, 1 - core], pair, one_send.at[2], one_recv.at[2], me + 1 - 2 * core, q)

    mixed_grad = product_of(sgrad[...], ow[...])
    out_og[...] = (mixed_grad * filtered[...]).astype(BF)
    fgrad[0:tokens, :] = mixed_grad * og[...].astype(F32)

    @pl.when(me > 0)
    def _():
        copy_to(fgrad.at[0:8], fgrad.at[tokens : tokens + 8], one_send.at[3], one_recv.at[3], me - 1, q)

    @pl.when(me == experts - 1)
    def _():
        fgrad[tokens : tokens + 8, :] = jnp.zeros((8, part_of(fgrad)), F32)

    wait_for(pair, one_recv.at[2])

    def pair_sum(m):
        at = rows_at(m, groups)
        psum[at] = (owp[at, core].astype(F32) + pair[at].astype(F32)).astype(BF)

    loop(0, chunks, pair_sum)

    def send_sum(k):
        to = lax.rem(here + k, pairs)
        copy_to(psum.at[to], arrived.at[here], one_send.at[4], one_recv.at[4], 2 * to + core, q)

    loop(1, pairs, send_sum)
    arrived[here] = psum[here]
    out_stream[...] = sgrad[:, mine]

    @pl.when(me < experts - 1)
    def _():
        wait_for(fgrad.at[tokens : tokens + 8], one_recv.at[3])

    product_grad = (
        taps[0:1, :] * fgrad[0:tokens, :] + taps[1:2, :] * fgrad[1 : tokens + 1, :] + taps[2:3, :] * fgrad[2 : tokens + 2, :]
    )
    out_ig[...] = (product_grad * ci[...].astype(F32)).astype(BF)
    out_ci[...] = (product_grad * ig[...].astype(F32)).astype(BF)

    def sent_rows(t):
        @pl.when((t >= 1) & (t < 6))
        def _():
            piece = rows.at[:, rows_at(0, span), mine]
            wait_for(piece, a_send.at[t])
            wait_for(piece, right_send.at[t])
            wait_for(piece, left_send.at[t])
            wait_for(rows.at[0, rows_at(0, span), mine], fright_send.at[t])
            wait_for(rows.at[0, rows_at(0, span), mine], fleft_send.at[t])

        @pl.when(t == 0)
        def _():
            if plane > 1:
                wait_for(rows.at[:, pl.ds(0, (plane - 1) * CAP), :], a_send.at[0])

        @pl.when(t >= 6)
        def _():
            wait_for(rows.at[:, rows_at(0, span), :], a_send.at[t])

        wait_for(summand.at[:, rows_at(0, span), :], rs_send.at[t])

    loop(0, 8, sent_rows)
    wait_for(back.at[pl.ds(0, (experts - 1) * CAP), :], one_send.at[1])
    for h in range(2):
        wait_for(tok.at[low, mine], tright_send.at[h])
        wait_for(tok.at[low, mine], tleft_send.at[h])
        wait_for(tok.at[low, mine], tf_send.at[h])
    wait_for(pair, one_send.at[2])

    @pl.when(me < experts - 1)
    def _():
        wait_for(extended.at[0:8], one_send.at[0])

    @pl.when(me > 0)
    def _():
        wait_for(fgrad.at[0:8], one_send.at[3])

    for copy in finished:
        copy.wait()
    wait_for(arrived.at[pl.ds(0, pairs - 1)], one_recv.at[4])
    added = arrived[0].astype(F32)
    for p in range(1, pairs):
        added = added + arrived[p].astype(F32)
    out_ow[...] = added
    wait_for(arrived.at[pl.ds(0, pairs - 1)], one_send.at[4])


def part_of(ref):
    return ref.shape[-1]


def whole_step(choice, scale, cot, stream, gain, og, ig, ci, taps, wg, wu, wd, ow, experts):
    tokens, width = cot.shape
    part = width // 4
    slots = experts * CAP
    plane = experts // 8
    hid = wg.shape[1]
    chan = og.shape[1]
    block = width // experts
    vm = pl.BlockSpec(memory_space=pltpu.VMEM)
    hbm = pl.BlockSpec(memory_space=pltpu.HBM)
    dma = pltpu.SemaphoreType.DMA
    return pl.pallas_call(
        functools.partial(step_kernel, plane),
        name="experts",
        out_shape=(
            jax.ShapeDtypeStruct((tokens, part), BF),
            jax.ShapeDtypeStruct((tokens, chan), BF),
            jax.ShapeDtypeStruct((tokens, chan), BF),
            jax.ShapeDtypeStruct((tokens, chan), BF),
            jax.ShapeDtypeStruct((block, chan), F32),
            jax.ShapeDtypeStruct((width, hid), BF),
            jax.ShapeDtypeStruct((width, hid), BF),
            jax.ShapeDtypeStruct((hid, width), BF),
        ),
        in_specs=[vm] * 9 + [hbm] * 4,
        out_specs=(vm,) * 5 + (hbm,) * 3,
        scratch_shapes=[
            pltpu.VMEM((width, hid), BF),
            pltpu.VMEM((width, hid), BF),
            pltpu.VMEM((hid, width), BF),
            pltpu.VMEM((width, chan), BF),
            pltpu.VMEM((tokens, 1), F32),
            pltpu.VMEM((tokens, width), BF),
            pltpu.VMEM((slots, tokens), BF),
            pltpu.VMEM((slots, 1), F32),
            pltpu.VMEM((3, 2, plane * CAP, width), BF),
            pltpu.VMEM((5, 2, plane * CAP, part), BF),
            pltpu.VMEM((2, slots, width), BF),
            pltpu.VMEM((slots, width), BF),
            pltpu.VMEM((3, slots, part), BF),
            pltpu.VMEM((slots, part), BF),
            pltpu.VMEM((slots, part), BF),
            pltpu.VMEM((slots, hid), BF),
            pltpu.VMEM((slots, hid), BF),
            pltpu.VMEM((slots, hid), BF),
            pltpu.VMEM((width, hid), BF),
            pltpu.VMEM((width, hid), BF),
            pltpu.VMEM((hid, width), BF),
            pltpu.VMEM((tokens, width), BF),
            pltpu.VMEM((tokens, width), BF),
            pltpu.VMEM((tokens + 8, chan), F32),
            pltpu.VMEM((tokens, chan), F32),
            pltpu.VMEM((tokens, chan), BF),
            pltpu.VMEM((tokens + 8, chan), F32),
            pltpu.VMEM((experts // 2, 2, block, chan), BF),
            pltpu.VMEM((experts // 2, block, chan), BF),
            pltpu.VMEM((experts // 2, block, chan), BF),
            pltpu.VMEM((experts // 2, block, chan), BF),
            dma((4,)),
            dma((3,)),
        ]
        + [dma((8,))] * 12
        + [dma((2,))] * 6
        + [dma((5,))] * 2,
        compiler_params=pltpu.CompilerParams(
            collective_id=0, has_side_effects=True, vmem_limit_bytes=62 * 1024 * 1024
        ),
    )(choice, scale, cot, stream, gain, og, ig, ci, taps, wg, wu, wd, ow)


def shards(
    cotangent,
    stream_in,
    norm_gain,
    out_gate,
    in_gate,
    conv_input,
    conv_taps,
    out_weight,
    expert_gate,
    expert_up,
    expert_down,
    expert_choice,
    route_scale,
):
    sp_size = lax.axis_size("sp")
    *others, grad_gate, grad_up, grad_down = whole_step(
        expert_choice.T, route_scale.T, cotangent, stream_in, norm_gain[None], out_gate, in_gate, conv_input, conv_taps,
        expert_gate[0], expert_up[0], expert_down[0], out_weight, sp_size,
    )
    return (*others, grad_gate[None].astype(F32), grad_up[None].astype(F32), grad_down[None].astype(F32))


def solution(mesh):
    placed = (
        P("sp", None),
        P("sp", None),
        P(),
        P("sp", "tp"),
        P("sp", "tp"),
        P("sp", "tp"),
        P(None, "tp"),
        P(None, "tp"),
        P("sp", None, "tp"),
        P("sp", None, "tp"),
        P("sp", "tp", None),
        P("sp", None),
        P("sp", None),
    )
    return jax.shard_map(
        shards,
        mesh=mesh,
        in_specs=placed,
        out_specs=(
            P("sp", "tp"),
            P("sp", "tp"),
            P("sp", "tp"),
            P("sp", "tp"),
            P("sp", "tp"),
            P("sp", None, "tp"),
            P("sp", None, "tp"),
            P("sp", "tp", None),
        ),
        check_vma=False,
    )
```

time: 222 us -> 177 us (0.80)
  starting transfers between devices: 22.7 us -> 0 us
  waiting for transfers between devices: 21.6 us -> 0 us
  Pallas kernels: 155 us -> 166 us
  local copies, waits for them, and re-layouts: 8.35 us -> 3.31 us
  other arithmetic: 10.5 us -> 5.53 us
  matrix products: 2.65 us -> 0 us
    all_to_all x1 -> x0, waiting for transfers between devices: 19.5 us -> none  [sent_and_summed(): lax.all_to_all(tiles, axis, split_axis=0, concat_axis=0, tiled=True)]
    all_to_all x1 -> x0, starting transfers between devices: 15.8 us -> none  [sent_and_summed(): lax.all_to_all(tiles, axis, split_axis=0, concat_axis=0, tiled=True)]
    pallas_call x1, Pallas kernels: 155 us -> 166 us  [whole_step(): pl.pallas_call(functools.partial(step_kernel, plane), name='experts', out...]
    ppermute x2 -> x0, starting transfers between devices: 6.93 us -> none  [passed_along(): lax.ppermute(value, axis, [(source, source + steps) for source in range(f...]
    reduce_sum x3 -> x0, other arithmetic: 4.53 us -> none  [the longest x1 2.24 us: shards(): along = jnp.mean(unit_stream * unit_grad, axis=-1, keepdims=True)]
    unnamed x23 -> x17, local copies, waits for them, and re-layouts: 6.91 us -> 3.31 us
    dot_general x2 -> x0, matrix products: 2.65 us -> none  [the longest x1 1.47 us: rows_product(): lax.dot_general(left, right, (((0,), (0,)), ((), ())), preferred_element_...]
    convert_element_type x3 -> x2, other arithmetic: 4.84 us -> 5.53 us  [the longest x1 3.97 us: shards(): grad_up[None].astype(F32)]
  transfers between devices with their start and end apart: 3 -> 0, of which waited for: 2 -> 0; matrix products, arithmetic and copies ran while one was open for 5% -> 0% of each run, Pallas kernels for 70% -> 0%
where the time goes in v2:
time: 177 us; the launch traced here: 176 us
  Pallas kernels  166 us (94%)
  other arithmetic  5.53 us (3%)
  local copies, waits for them, and re-layouts  3.31 us (2%)
    pallas_call x1, Pallas kernels, whole_step(): pl.pallas_call(functools.partial(step_kernel, plane), name='experts', out...  166 us
    convert_element_type x1, other arithmetic, shards(): grad_up[None].astype(F32)  3.97 us

profile of v2, /device:TPU:1, one launch (start us, length us, event | category | flops | bytes accessed | tf_op | source)
XLA Modules:
  0.0 175.9 jit_solution(10703890165415401664)
XLA Ops:
  0.6 166.3 %experts.1 = (bf16[256,512]{1,0:T(8,128)(2,1)}, bf16[256,256]{1,0:T(8,128)(2,1)}, bf16[256,256]{1,0:T(8,128)(2,1)}, bf16[256,256]{1,0:T(8,128)(2,1)}, f32[32,256...) custom-call(s32[2,256]{1,0:T(2,128)} %bitcast.19, ...), custom_call_target="tpu_custom_call" | custom-call | tf_op jit(solution)/shard_map/experts/pallas_call | solution.py:458
  167.0 0.0 copy-start
  167.0 4.0 %bitcast_convert_fusion.1 = (f32[1,2048,256]{2,1,0:T(8,128)}, f32[1,2048,256]{2,1,0:T(8,128)}) fusion(bf16[2048,256]{1,0:T(8,128)(2,1)} %get-tuple-element.22, bf16[2048,256]{1,0:T(8,128)(2,1)} %get-tuple-element.21), kind=kLoop, calls=%fused_computation.1 | loop fusion | flops 1048576 | bytes 6291456 | tf_op jit(solution)/shard_map/convert_element_type | solution.py:537
  171.0 0.0 copy-start.1
  171.0 0.0 copy-start.4
  171.0 0.0 copy-start.3
  171.0 0.0 copy-done
  171.0 0.0 copy-start.2
  171.0 0.0 copy-start.5
  171.0 1.6 bitcast_convert_fusion
  172.6 0.0 copy-done.1
  172.6 0.7 copy.26
  173.3 0.0 copy-done.4
  173.3 0.7 copy.27
  173.9 0.0 copy-done.3
  173.9 0.7 copy.28
  174.6 0.0 copy-done.2
  174.6 0.7 copy.29
  175.2 0.0 copy-done.5
  175.3 0.6 copy.30
Async XLA Ops:
  167.0 4.0 %copy-start = (bf16[256,2048]{1,0:T(8,128)(2,1)S(1)}, bf16[256,2048]{1,0:T(8,128)(2,1)}, u32[]{:S(2)}) copy-start(bf16[256,2048]{1,0:T(8,128)(2,1)} %get-tuple-element.23) | copy-start | bytes 3145732
  171.0 1.6 copy-start.1
  171.0 2.3 %copy-start.4 = (bf16[256,256]{1,0:T(8,128)(2,1)S(1)}, bf16[256,256]{1,0:T(8,128)(2,1)}, u32[]{:S(2)}) copy-start(bf16[256,256]{1,0:T(8,128)(2,1)} %get-tuple-element.35) | copy-start | bytes 393220
  171.0 3.0 %copy-start.3 = (bf16[256,256]{1,0:T(8,128)(2,1)S(1)}, bf16[256,256]{1,0:T(8,128)(2,1)}, u32[]{:S(2)}) copy-start(bf16[256,256]{1,0:T(8,128)(2,1)} %get-tuple-element.36) | copy-start | bytes 393220
  171.0 3.6 %copy-start.2 = (bf16[256,256]{1,0:T(8,128)(2,1)S(1)}, bf16[256,256]{1,0:T(8,128)(2,1)}, u32[]{:S(2)}) copy-start(bf16[256,256]{1,0:T(8,128)(2,1)} %get-tuple-element.37) | copy-start | bytes 393220
  171.0 4.3 %copy-start.5 = (f32[32,256]{1,0:T(8,128)S(1)}, f32[32,256]{1,0:T(8,128)}, u32[]{:S(2)}) copy-start(f32[32,256]{1,0:T(8,128)} %get-tuple-element.38) | copy-start | bytes 98308

commit v3 on v2

--- a/solution.py
+++ b/solution.py
@@ -50,11 +50,11 @@
     out_stream, out_og, out_ig, out_ci, out_ow, out_gate, out_up, out_down,
     wg, wu, wd, ow, inverse, normed, pick, weight, send_all, send_part, rows, partial, summand, total, back,
     hidden, ggrad, ugrad, gate_out, up_out, down_out, tok, sgrad, extended, filtered, mixed, fgrad,
-    owp, pair, psum, arrived,
+    owp, pair, psum, arrived, gate_sum, up_sum, down_sum,
     in_sem, out_sem,
     a_send, a_recv, right_send, left_send, from_left, from_right,
     fright_send, fleft_send, ffrom_left, ffrom_right,
-    rs_send, rs_recv, tright_send, tleft_send, tfrom_left, tfrom_right, tf_send, tf_recv, one_send, one_recv,
+    rs_send, rs_recv, tright_send, tleft_send, tfrom_left, tfrom_right, tf_send, tf_recv, one_send, one_recv, pair_send, pair_recv,
 ):
     me = lax.axis_index("sp")
     q = lax.axis_index("tp")
@@ -143,20 +143,6 @@
 
     loop(1, 6, fill_quarter)
 
-    def turn_of(i):
-        return i + 5 * lax.div(i + 1, 2)
-
-    def fill_whole(i):
-        at = rows_at(lax.rem(z + offset_of(turn_of(i)), 8), span)
-        chosen = pick[at, :]
-        send_all[i, 0] = product_of(chosen, normed[...]).astype(BF)
-        send_all[i, 1] = (product_of(chosen, cot[...]) * weight[at, :]).astype(BF)
-
-    loop(0, 3, fill_whole)
-    own = rows_at(place, CAP)
-    rows[0, my_slots, :] = send_all[0, 0, own, :]
-    rows[1, my_slots, :] = send_all[0, 1, own, :]
-
     extended[8 : tokens + 8, :] = ig[...].astype(F32) * ci[...].astype(F32)
 
     @pl.when(me == 0)
@@ -182,6 +168,20 @@
         loop(0, plane, one)
 
     loop(1, 6, send_quarter)
+
+    def turn_of(i):
+        return i + 5 * lax.div(i + 1, 2)
+
+    def fill_whole(i):
+        at = rows_at(lax.rem(z + offset_of(turn_of(i)), 8), span)
+        chosen = pick[at, :]
+        send_all[i, 0] = product_of(chosen, normed[...]).astype(BF)
+        send_all[i, 1] = (product_of(chosen, cot[...]) * weight[at, :]).astype(BF)
+
+    loop(0, 3, fill_whole)
+    own = rows_at(place, CAP)
+    rows[0, my_slots, :] = send_all[0, 0, own, :]
+    rows[1, my_slots, :] = send_all[0, 1, own, :]
 
     def send_whole(i):
         t = turn_of(i)
@@ -212,6 +212,15 @@
     )
     filtered[...] = now
     mixed[...] = (og[...].astype(F32) * now).astype(BF)
+    chunk = min(256, width)
+
+    def clear(m):
+        cols = rows_at(m, chunk)
+        gate_sum[cols, :] = jnp.zeros((chunk, part_of(gate_sum)), F32)
+        up_sum[cols, :] = jnp.zeros((chunk, part_of(up_sum)), F32)
+        down_sum[:, cols] = jnp.zeros((down_sum.shape[0], chunk), F32)
+
+    loop(0, width // chunk, clear)
     for copy in weights:
         copy.wait()
 
@@ -234,9 +243,9 @@
             half = rows.at[1, at, of_right]
             copy_to(half, half, fleft_send.at[t], ffrom_right.at[t], me, left)
 
-        @pl.when((i == 0) | ((i >= 3) & (i < 10)))
+        @pl.when((i >= 2) & (i < 10))
         def _():
-            t = (i - 2) * lax.div(i + 13, 16)
+            t = i - 2
             at = rows_at(source_at(t), span)
 
             @pl.when((t >= 1) & (t < 6))
@@ -272,6 +281,15 @@
 
             loop(1, 4, one)
 
+            def add_grads(m):
+                cols = rows_at(m, chunk)
+                rows_here = rows[0, at, cols]
+                gate_sum[cols, :] += rows_product(rows_here, ggrad[at, :])
+                up_sum[cols, :] += rows_product(rows_here, ugrad[at, :])
+                down_sum[:, cols] += rows_product(hidden[at, :], rows[1, at, cols])
+
+            loop(0, width // chunk, add_grads)
+
         @pl.when(i >= 3)
         def _():
             t = i - 3
@@ -292,19 +310,16 @@
 
             loop(0, plane, one)
 
-    loop(0, 11, step)
+    loop(1, 11, step)
     back[my_slots, :] = total[my_slots, :]
 
-    chunk = min(256, width)
-
-    def grads(m):
+    def narrow(m):
         cols = rows_at(m, chunk)
-        here = rows[0, :, cols]
-        gate_out[cols, :] = rows_product(here, ggrad[...]).astype(BF)
-        up_out[cols, :] = rows_product(here, ugrad[...]).astype(BF)
-        down_out[:, cols] = rows_product(hidden[...], rows[1, :, cols]).astype(BF)
-
-    loop(0, width // chunk, grads)
+        gate_out[cols, :] = gate_sum[cols, :].astype(BF)
+        up_out[cols, :] = up_sum[cols, :].astype(BF)
+        down_out[:, cols] = down_sum[:, cols].astype(BF)
+
+    loop(0, width // chunk, narrow)
     finished = (
         pltpu.make_async_copy(gate_out, out_gate, out_sem.at[0]),
         pltpu.make_async_copy(up_out, out_up, out_sem.at[1]),
@@ -344,43 +359,52 @@
     pairs = experts // 2
     core = lax.rem(me, 2)
     here = lax.div(me, 2)
-    chunks = min(8, pairs)
-    groups = pairs // chunks
-    cut = 2 * groups * block
-
-    def out_rows(m):
-        found = rows_product(sgrad[:, rows_at(m, cut)], mixed[...]).astype(BF)
-        owp[rows_at(m, groups)] = found.reshape(groups, 2, block, found.shape[-1])
-
-    loop(0, chunks, out_rows)
-    copy_to(owp.at[:, 1 - core], pair, one_send.at[2], one_recv.at[2], me + 1 - 2 * core, q)
+    groups = plane // 2
+    cut = plane * block
+
+    def plane_of(j):
+        half = lax.div(j + 1, 2)
+        return lax.rem(z + 4 + half - 2 * half * lax.rem(j, 2), 8)
+
+    def out_rows(j):
+        at = plane_of(j)
+        found = rows_product(sgrad[:, rows_at(at, cut)], mixed[...]).astype(BF)
+        of_plane = rows_at(at, groups)
+        owp[of_plane] = found.reshape(groups, 2, block, found.shape[-1])
+        copy_to(owp.at[of_plane, 1 - core], pair.at[of_plane], pair_send.at[j], pair_recv.at[j], me + 1 - 2 * core, q)
+
+    loop(0, 8, out_rows)
+
+    def pair_sum(j):
+        at = plane_of(j)
+        of_plane = rows_at(at, groups)
+        wait_for(pair.at[of_plane], pair_recv.at[j])
+        psum[of_plane] = (owp[of_plane, core].astype(F32) + pair[of_plane].astype(F32)).astype(BF)
+
+        def send_sum(k):
+            to = at * groups + lax.rem(here + k, groups)
+
+            @pl.when(to != here)
+            def _():
+                copy_to(psum.at[to], arrived.at[here], one_send.at[4], one_recv.at[4], 2 * to + core, q)
+
+        loop(0, groups, send_sum)
+
+    loop(0, 8, pair_sum)
+    arrived[here] = psum[here]
 
     mixed_grad = product_of(sgrad[...], ow[...])
+    fgrad[0:tokens, :] = mixed_grad * og[...].astype(F32)
+
+    @pl.when(me > 0)
+    def _():
+        copy_to(fgrad.at[0:8], fgrad.at[tokens : tokens + 8], one_send.at[3], one_recv.at[3], me - 1, q)
+
+    @pl.when(me == experts - 1)
+    def _():
+        fgrad[tokens : tokens + 8, :] = jnp.zeros((8, part_of(fgrad)), F32)
+
     out_og[...] = (mixed_grad * filtered[...]).astype(BF)
-    fgrad[0:tokens, :] = mixed_grad * og[...].astype(F32)
-
-    @pl.when(me > 0)
-    def _():
-        copy_to(fgrad.at[0:8], fgrad.at[tokens : tokens + 8], one_send.at[3], one_recv.at[3], me - 1, q)
-
-    @pl.when(me == experts - 1)
-    def _():
-        fgrad[tokens : tokens + 8, :] = jnp.zeros((8, part_of(fgrad)), F32)
-
-    wait_for(pair, one_recv.at[2])
-
-    def pair_sum(m):
-        at = rows_at(m, groups)
-        psum[at] = (owp[at, core].astype(F32) + pair[at].astype(F32)).astype(BF)
-
-    loop(0, chunks, pair_sum)
-
-    def send_sum(k):
-        to = lax.rem(here + k, pairs)
-        copy_to(psum.at[to], arrived.at[here], one_send.at[4], one_recv.at[4], 2 * to + core, q)
-
-    loop(1, pairs, send_sum)
-    arrived[here] = psum[here]
     out_stream[...] = sgrad[:, mine]
 
     @pl.when(me < experts - 1)
@@ -420,7 +444,11 @@
         wait_for(tok.at[low, mine], tright_send.at[h])
         wait_for(tok.at[low, mine], tleft_send.at[h])
         wait_for(tok.at[low, mine], tf_send.at[h])
-    wait_for(pair, one_send.at[2])
+
+    def pair_sent(j):
+        wait_for(pair.at[pl.ds(0, groups)], pair_send.at[j])
+
+    loop(0, 8, pair_sent)
 
     @pl.when(me < experts - 1)
     def _():
@@ -502,16 +530,40 @@
             pltpu.VMEM((experts // 2, block, chan), BF),
             pltpu.VMEM((experts // 2, block, chan), BF),
             pltpu.VMEM((experts // 2, block, chan), BF),
+            pltpu.VMEM((width, hid), F32),
+            pltpu.VMEM((width, hid), F32),
+            pltpu.VMEM((hid, width), F32),
             dma((4,)),
             dma((3,)),
         ]
         + [dma((8,))] * 12
         + [dma((2,))] * 6
-        + [dma((5,))] * 2,
+        + [dma((5,))] * 2
+        + [dma((8,))] * 2,
         compiler_params=pltpu.CompilerParams(
             collective_id=0, has_side_effects=True, vmem_limit_bytes=62 * 1024 * 1024
         ),
     )(choice, scale, cot, stream, gain, og, ig, ci, taps, wg, wu, wd, ow)
+
+
+def finish_kernel(*refs):
+    half = len(refs) // 2
+    for given, out in zip(refs[:half], refs[half:]):
+        out[...] = given[...].astype(out.dtype)
+
+
+def finished_outputs(arrays, steps):
+    types = [F32 if k > 3 else BF for k in range(len(arrays))]
+    specs = [pl.BlockSpec((a.shape[0] // steps, a.shape[1]), lambda i: (i, 0)) for a in arrays]
+    specs[4] = pl.BlockSpec(arrays[4].shape, lambda i: (0, 0))
+    return pl.pallas_call(
+        finish_kernel,
+        name="finish",
+        grid=(steps,),
+        out_shape=[jax.ShapeDtypeStruct(a.shape, t) for a, t in zip(arrays, types)],
+        in_specs=specs,
+        out_specs=specs,
+    )(*arrays)
 
 
 def shards(
@@ -530,11 +582,12 @@
     route_scale,
 ):
     sp_size = lax.axis_size("sp")
-    *others, grad_gate, grad_up, grad_down = whole_step(
+    arrays = whole_step(
         expert_choice.T, route_scale.T, cotangent, stream_in, norm_gain[None], out_gate, in_gate, conv_input, conv_taps,
         expert_gate[0], expert_up[0], expert_down[0], out_weight, sp_size,
     )
-    return (*others, grad_gate[None].astype(F32), grad_up[None].astype(F32), grad_down[None].astype(F32))
+    *others, grad_gate, grad_up, grad_down = finished_outputs(arrays, 4)
+    return (*others, grad_gate[None], grad_up[None], grad_down[None])
 
 
 def solution(mesh):

time: 177 us -> 164 us (0.927)
  other arithmetic: 5.53 us -> 0 us
  local copies, waits for them, and re-layouts: 3.31 us -> 0 us
  Pallas kernels: 166 us -> 163 us
    pallas_call x1, Pallas kernels: 166 us -> 158 us  [whole_step(): pl.pallas_call(functools.partial(step_kernel, plane), name='experts', out...]
    convert_element_type x2 -> x0, other arithmetic: 5.53 us -> none  [the longest x1 3.97 us: shards(): grad_up[None].astype(F32)]
    pallas_call x0 -> x1, Pallas kernels: none -> 5.37 us  [finished_outputs(): pl.pallas_call(finish_kernel, name='finish', grid=(steps,), out_shape=[ja...]
    unnamed x17 -> x0, local copies, waits for them, and re-layouts: 3.31 us -> none
where the time goes in v3:
time: 164 us
  Pallas kernels  163 us (99%)
    pallas_call x1, Pallas kernels, whole_step(): pl.pallas_call(functools.partial(step_kernel, plane), name='experts', out...  158 us
    pallas_call x1, Pallas kernels, finished_outputs(): pl.pallas_call(finish_kernel, name='finish', grid=(steps,), out_shape=[ja...  5.37 us

profile of v3, /device:TPU:1, one launch (start us, length us, event | category | flops | bytes accessed | tf_op | source)
XLA Modules:
  0.0 163.7 jit_solution(1911459442663217484)
XLA Ops:
  0.6 157.6 %experts.1 = (bf16[256,512]{1,0:T(8,128)(2,1)}, bf16[256,256]{1,0:T(8,128)(2,1)}, bf16[256,256]{1,0:T(8,128)(2,1)}, bf16[256,256]{1,0:T(8,128)(2,1)}, f32[32,256...) custom-call(s32[2,256]{1,0:T(2,128)} %bitcast.13, ...), custom_call_target="tpu_custom_call" | custom-call | tf_op jit(solution)/shard_map/experts/pallas_call | solution.py:486
  158.3 5.4 %finish.1 = (bf16[256,512]{1,0:T(8,128)(2,1)}, bf16[256,256]{1,0:T(8,128)(2,1)}, bf16[256,256]{1,0:T(8,128)(2,1)}, bf16[256,256]{1,0:T(8,128)(2,1)}, f32[32,256]...) custom-call(bf16[256,512]{1,0:T(8,128)(2,1)} %get-tuple-element.24.refs_0_, ...), custom_call_target="tpu_custom_call" | custom-call | tf_op jit(solution)/shard_map/finish/pallas_call | solution.py:559

commit v4 on v3

--- a/solution.py
+++ b/solution.py
@@ -46,16 +46,20 @@
 
 
 def step_kernel(
-    plane, choice, scale, cot, stream, gain, og, ig, ci, taps, wg_hbm, wu_hbm, wd_hbm, ow_hbm,
-    out_stream, out_og, out_ig, out_ci, out_ow, out_gate, out_up, out_down,
-    wg, wu, wd, ow, inverse, normed, pick, weight, send_all, send_part, rows, partial, summand, total, back,
-    hidden, ggrad, ugrad, gate_out, up_out, down_out, tok, sgrad, extended, filtered, mixed, fgrad,
-    owp, pair, psum, arrived, gate_sum, up_sum, down_sum,
-    in_sem, out_sem,
-    a_send, a_recv, right_send, left_send, from_left, from_right,
-    fright_send, fleft_send, ffrom_left, ffrom_right,
-    rs_send, rs_recv, tright_send, tleft_send, tfrom_left, tfrom_right, tf_send, tf_recv, one_send, one_recv, pair_send, pair_recv,
+    plane, choice, scale, gain, taps, stream_hbm, cot_hbm, ig_hbm, ci_hbm, og_hbm, wg_hbm, wu_hbm, wd_hbm, ow_hbm,
+    *refs,
 ):
+    outs, refs = refs[:8], refs[8:]
+    (
+        stream, cot, ig, ci, og, wg, wu, wd, ow, inverse, normed, pick, weight, send_all, send_part, rows, partial, summand, far_in, far_sum, total, back,
+        hidden, ggrad, ugrad, gate_out, up_out, down_out, tok, sgrad, extended, filtered, mixed, fgrad,
+        owp, pair, psum, arrived, gate_sum, up_sum, down_sum,
+        stream_out, og_out, ig_out, ci_out, ow_out,
+        in_sem, out_sem,
+        a_send, a_recv, half_recv, right_send, left_send, from_left, from_right,
+        fright_send, fleft_send, ffrom_left, ffrom_right,
+        rs_send, far_send, of_left_recv, of_right_recv, far_left_recv, far_right_recv, tright_send, tleft_send, tfrom_left, tfrom_right, tf_send, tf_recv, one_send, one_recv, pair_send, pair_recv,
+    ) = refs
     me = lax.axis_index("sp")
     q = lax.axis_index("tp")
     right = lax.rem(q + 1, 4)
@@ -84,13 +88,10 @@
     def next_place(k):
         return lax.rem(place + k, plane)
 
-    weights = (
-        pltpu.make_async_copy(wg_hbm, wg, in_sem.at[0]),
-        pltpu.make_async_copy(wu_hbm, wu, in_sem.at[1]),
-        pltpu.make_async_copy(wd_hbm, wd, in_sem.at[2]),
-        pltpu.make_async_copy(ow_hbm, ow, in_sem.at[3]),
-    )
-    for copy in weights:
+    given = (stream_hbm, cot_hbm, ig_hbm, ci_hbm, og_hbm, wg_hbm, wu_hbm, wd_hbm, ow_hbm)
+    held = (stream, cot, ig, ci, og, wg, wu, wd, ow)
+    copies = [pltpu.make_async_copy(a, b, in_sem.at[n]) for n, (a, b) in enumerate(zip(given, held))]
+    for copy in copies:
         copy.start()
 
     barrier = pltpu.get_barrier_semaphore()
@@ -104,15 +105,6 @@
         pl.semaphore_signal(barrier, inc=1, device_id=(me, lax.rem(q + k, 4)), device_id_type=MESH)
 
     loop(1, 4, greet_row)
-
-    def norm_rows(r):
-        at = rows_at(r, 16)
-        x = stream[at, :].astype(F32)
-        inv = lax.rsqrt(jnp.mean(x * x, axis=-1, keepdims=True) + norm_eps)
-        inverse[at, :] = inv
-        normed[at, :] = ((x * inv) * gain[...]).astype(BF)
-
-    loop(0, tokens // 16, norm_rows)
 
     first, second = choice[0:1, :], choice[1:2, :]
     ids = lax.broadcasted_iota(jnp.int32, (experts, tokens), 0)
@@ -135,6 +127,19 @@
 
     loop(0, 8, pick_rows)
 
+    copies[0].wait()
+
+    def norm_rows(r):
+        at = rows_at(r, 32)
+        x = stream[at, :].astype(F32)
+        inv = lax.rsqrt(jnp.mean(x * x, axis=-1, keepdims=True) + norm_eps)
+        inverse[at, :] = inv
+        normed[at, :] = ((x * inv) * gain[...]).astype(BF)
+
+    loop(0, tokens // 32, norm_rows)
+
+    copies[1].wait()
+
     def fill_quarter(t):
         at = rows_at(lax.rem(z + offset_of(t), 8), span)
         chosen = pick[at, :]
@@ -143,6 +148,8 @@
 
     loop(1, 6, fill_quarter)
 
+    copies[2].wait()
+    copies[3].wait()
     extended[8 : tokens + 8, :] = ig[...].astype(F32) * ci[...].astype(F32)
 
     @pl.when(me == 0)
@@ -154,15 +161,19 @@
     @pl.when(me < experts - 1)
     def _():
         copy_to(extended.at[tokens : tokens + 8], extended.at[0:8], one_send.at[0], one_recv.at[0], me + 1, q)
+
+    side = plane // 2
 
     def send_quarter(t):
         target = lax.rem(z + offset_of(t), 8)
 
         def one(k):
-            to = next_place(k)
+            turn = lax.div(k, side)
+            block = lax.rem(lax.div(place, side) + turn, 2)
+            to = block * side + lax.rem(place + k, side)
             copy_to(
                 send_part.at[t - 1, :, rows_at(to, CAP), :], rows.at[:, my_slots, mine],
-                a_send.at[t], a_recv.at[t], target * plane + to, q,
+                a_send.at[t], half_recv.at[2 * t + turn], target * plane + to, q,
             )
 
         loop(0, plane, one)
@@ -199,12 +210,14 @@
 
         loop(0, plane, one)
 
-    loop(0, 3, send_whole)
+
+    send_whole(0)
 
     @pl.when(me > 0)
     def _():
         wait_for(extended.at[0:8], one_recv.at[0])
 
+    copies[4].wait()
     now = (
         taps[0:1, :] * extended[8 : tokens + 8, :]
         + taps[1:2, :] * extended[7 : tokens + 7, :]
@@ -221,16 +234,47 @@
         down_sum[:, cols] = jnp.zeros((down_sum.shape[0], chunk), F32)
 
     loop(0, width // chunk, clear)
-    for copy in weights:
+    for copy in copies[5:]:
         copy.wait()
+
+    def add_grads(at):
+        def one(m):
+            cols = rows_at(m, chunk)
+            here = rows[0, at, cols]
+            gate_sum[cols, :] += rows_product(here, ggrad[at, :])
+            up_sum[cols, :] += rows_product(here, ugrad[at, :])
+            down_sum[:, cols] += rows_product(hidden[at, :], rows[1, at, cols])
+
+        loop(0, width // chunk, one)
+
+    def halves_at(t):
+        source = source_at(t)
+        return rows_at(2 * source, span // 2), rows_at(2 * source + 1, span // 2), source
+
+    def pass_sum(t):
+        upper, lower, source = halves_at(t)
+        held_at = rows_at(source, span // 2)
+        wait_for(far_in.at[0, held_at, :], far_left_recv.at[t])
+        far_sum[0, held_at, :] = (partial[upper, of_right].astype(F32) + far_in[0, held_at, :].astype(F32)).astype(BF)
+        copy_to(far_sum.at[0, held_at, :], summand.at[0, upper, :], rs_send.at[t], of_left_recv.at[t], me, right)
+        wait_for(far_in.at[1, held_at, :], far_right_recv.at[t])
+        far_sum[1, held_at, :] = (partial[lower, of_left].astype(F32) + far_in[1, held_at, :].astype(F32)).astype(BF)
+        copy_to(far_sum.at[1, held_at, :], summand.at[1, lower, :], rs_send.at[t], of_right_recv.at[t], me, left)
 
     def step(i):
         @pl.when((i >= 1) & (i < 6))
         def _():
-            piece = rows.at[:, rows_at(source_at(i), span), mine]
-            wait_for(piece, a_recv.at[i])
-            copy_to(piece, piece, right_send.at[i], from_left.at[i], me, right)
-            copy_to(piece, piece, left_send.at[i], from_right.at[i], me, left)
+            for turn in range(2):
+                block = lax.rem(lax.div(place, side) + turn, 2)
+                piece = rows.at[:, rows_at(2 * source_at(i) + block, span // 2), mine]
+                wait_for(piece, half_recv.at[2 * i + turn])
+                copy_to(piece, piece, right_send.at[i], from_left.at[i], me, right)
+                copy_to(piece, piece, left_send.at[i], from_right.at[i], me, left)
+
+        @pl.when(i == 3)
+        def _():
+            send_whole(1)
+            send_whole(2)
 
         @pl.when((i >= 2) & (i < 7))
         def _():
@@ -242,6 +286,10 @@
             wait_for(rows.at[:, at, of_right], from_right.at[t])
             half = rows.at[1, at, of_right]
             copy_to(half, half, fleft_send.at[t], ffrom_right.at[t], me, left)
+
+        @pl.when((i >= 3) & (i < 8))
+        def _():
+            pass_sum(i - 3)
 
         @pl.when((i >= 2) & (i < 10))
         def _():
@@ -275,30 +323,29 @@
             ugrad[at, :] = up_grad
             partial[at, :] = (cols_product(gate_grad, wg[...]) + cols_product(up_grad, wu[...])).astype(BF)
 
-            def one(d):
-                to = lax.rem(q + d, 4)
-                copy_to(partial.at[at, rows_at(to, part)], summand.at[d - 1, at, :], rs_send.at[t], rs_recv.at[t], me, to)
-
-            loop(1, 4, one)
-
-            def add_grads(m):
-                cols = rows_at(m, chunk)
-                rows_here = rows[0, at, cols]
-                gate_sum[cols, :] += rows_product(rows_here, ggrad[at, :])
-                up_sum[cols, :] += rows_product(rows_here, ugrad[at, :])
-                down_sum[:, cols] += rows_product(hidden[at, :], rows[1, at, cols])
-
-            loop(0, width // chunk, add_grads)
-
-        @pl.when(i >= 3)
-        def _():
-            t = i - 3
+            upper, lower, source = halves_at(t)
+            held_at = rows_at(source, span // 2)
+            copy_to(partial.at[upper, of_far], far_in.at[0, held_at, :], far_send.at[t], far_left_recv.at[t], me, right)
+            copy_to(partial.at[lower, of_far], far_in.at[1, held_at, :], far_send.at[t], far_right_recv.at[t], me, left)
+            copy_to(partial.at[lower, of_right], summand.at[0, lower, :], rs_send.at[t], of_left_recv.at[t], me, right)
+            copy_to(partial.at[upper, of_left], summand.at[1, upper, :], rs_send.at[t], of_right_recv.at[t], me, left)
+
+            @pl.when(t < 6)
+            def _():
+                add_grads(at)
+
+        @pl.when((i >= 8) & (i < 11))
+        def _():
+            pass_sum(i - 3)
+
+        @pl.when(i >= 4)
+        def _():
+            t = i - 4
             source = source_at(t)
             at = rows_at(source, span)
-            wait_for(summand.at[:, at, :], rs_recv.at[t])
-            added = partial[at, mine].astype(F32)
-            for d in range(3):
-                added = added + summand[d, at, :].astype(F32)
+            wait_for(summand.at[0, at, :], of_left_recv.at[t])
+            wait_for(summand.at[1, at, :], of_right_recv.at[t])
+            added = partial[at, mine].astype(F32) + summand[0, at, :].astype(F32) + summand[1, at, :].astype(F32)
             total[at, :] = added.astype(BF)
 
             def one(k):
@@ -310,23 +357,13 @@
 
             loop(0, plane, one)
 
-    loop(1, 11, step)
+    loop(1, 12, step)
     back[my_slots, :] = total[my_slots, :]
 
-    def narrow(m):
-        cols = rows_at(m, chunk)
-        gate_out[cols, :] = gate_sum[cols, :].astype(BF)
-        up_out[cols, :] = up_sum[cols, :].astype(BF)
-        down_out[:, cols] = down_sum[:, cols].astype(BF)
-
-    loop(0, width // chunk, narrow)
-    finished = (
-        pltpu.make_async_copy(gate_out, out_gate, out_sem.at[0]),
-        pltpu.make_async_copy(up_out, out_up, out_sem.at[1]),
-        pltpu.make_async_copy(down_out, out_down, out_sem.at[2]),
-    )
-    for copy in finished:
-        copy.start()
+    def late_grads(t):
+        add_grads(rows_at(source_at(t), span))
+
+    loop(6, 7, late_grads)
 
     wait_for(back.at[pl.ds(0, (experts - 1) * CAP), :], one_recv.at[1])
     tok[:, mine] = rows_product(pick[...], back[...]).astype(BF)
@@ -336,10 +373,23 @@
         copy_to(tok.at[at, mine], tok.at[at, mine], tright_send.at[h], tfrom_left.at[h], me, right)
     for h, at in ((1, high), (0, low)):
         copy_to(tok.at[at, mine], tok.at[at, mine], tleft_send.at[h], tfrom_right.at[h], me, left)
+    loop(7, 8, late_grads)
     wait_for(tok.at[low, of_left], tfrom_left.at[0])
     copy_to(tok.at[low, of_left], tok.at[low, of_left], tf_send.at[0], tf_recv.at[0], me, right)
     wait_for(tok.at[high, of_right], tfrom_right.at[1])
     copy_to(tok.at[high, of_right], tok.at[high, of_right], tf_send.at[1], tf_recv.at[1], me, left)
+    def narrow(m):
+        cols = rows_at(m, chunk)
+        gate_out[cols, :] = gate_sum[cols, :].astype(BF)
+        up_out[cols, :] = up_sum[cols, :].astype(BF)
+        down_out[:, cols] = down_sum[:, cols].astype(BF)
+
+    loop(0, width // chunk, narrow)
+    ready = (stream_out, og_out, ig_out, ci_out, ow_out, gate_out, up_out, down_out)
+    finished = [pltpu.make_async_copy(a, b, out_sem.at[n]) for n, (a, b) in enumerate(zip(ready, outs))]
+    for copy in finished[5:]:
+        copy.start()
+
     wait_for(tok.at[high, of_left], tfrom_left.at[1])
     wait_for(tok.at[low, of_right], tfrom_right.at[0])
     wait_for(tok.at[low, of_far], tf_recv.at[0])
@@ -404,8 +454,10 @@
     def _():
         fgrad[tokens : tokens + 8, :] = jnp.zeros((8, part_of(fgrad)), F32)
 
-    out_og[...] = (mixed_grad * filtered[...]).astype(BF)
-    out_stream[...] = sgrad[:, mine]
+    og_out[...] = (mixed_grad * filtered[...]).astype(BF)
+    finished[1].start()
+    stream_out[...] = sgrad[:, mine]
+    finished[0].start()
 
     @pl.when(me < experts - 1)
     def _():
@@ -414,8 +466,10 @@
     product_grad = (
         taps[0:1, :] * fgrad[0:tokens, :] + taps[1:2, :] * fgrad[1 : tokens + 1, :] + taps[2:3, :] * fgrad[2 : tokens + 2, :]
     )
-    out_ig[...] = (product_grad * ci[...].astype(F32)).astype(BF)
-    out_ci[...] = (product_grad * ig[...].astype(F32)).astype(BF)
+    ig_out[...] = (product_grad * ci[...].astype(F32)).astype(BF)
+    ci_out[...] = (product_grad * ig[...].astype(F32)).astype(BF)
+    finished[2].start()
+    finished[3].start()
 
     def sent_rows(t):
         @pl.when((t >= 1) & (t < 6))
@@ -437,6 +491,7 @@
             wait_for(rows.at[:, rows_at(0, span), :], a_send.at[t])
 
         wait_for(summand.at[:, rows_at(0, span), :], rs_send.at[t])
+        wait_for(summand.at[0, rows_at(0, span), :], far_send.at[t])
 
     loop(0, 8, sent_rows)
     wait_for(back.at[pl.ds(0, (experts - 1) * CAP), :], one_send.at[1])
@@ -458,13 +513,14 @@
     def _():
         wait_for(fgrad.at[0:8], one_send.at[3])
 
-    for copy in finished:
-        copy.wait()
     wait_for(arrived.at[pl.ds(0, pairs - 1)], one_recv.at[4])
     added = arrived[0].astype(F32)
     for p in range(1, pairs):
         added = added + arrived[p].astype(F32)
-    out_ow[...] = added
+    ow_out[...] = added
+    finished[4].start()
+    for copy in finished:
+        copy.wait()
     wait_for(arrived.at[pl.ds(0, pairs - 1)], one_send.at[4])
 
 
@@ -472,7 +528,7 @@
     return ref.shape[-1]
 
 
-def whole_step(choice, scale, cot, stream, gain, og, ig, ci, taps, wg, wu, wd, ow, experts):
+def whole_step(choice, scale, gain, taps, stream, cot, ig, ci, og, wg, wu, wd, ow, experts):
     tokens, width = cot.shape
     part = width // 4
     slots = experts * CAP
@@ -496,9 +552,14 @@
             jax.ShapeDtypeStruct((width, hid), BF),
             jax.ShapeDtypeStruct((hid, width), BF),
         ),
-        in_specs=[vm] * 9 + [hbm] * 4,
-        out_specs=(vm,) * 5 + (hbm,) * 3,
+        in_specs=[vm] * 4 + [hbm] * 9,
+        out_specs=(hbm,) * 8,
         scratch_shapes=[
+            pltpu.VMEM((tokens, width), BF),
+            pltpu.VMEM((tokens, width), BF),
+            pltpu.VMEM((tokens, chan), BF),
+            pltpu.VMEM((tokens, chan), BF),
+            pltpu.VMEM((tokens, chan), BF),
             pltpu.VMEM((width, hid), BF),
             pltpu.VMEM((width, hid), BF),
             pltpu.VMEM((hid, width), BF),
@@ -511,7 +572,9 @@
             pltpu.VMEM((5, 2, plane * CAP, part), BF),
             pltpu.VMEM((2, slots, width), BF),
             pltpu.VMEM((slots, width), BF),
-            pltpu.VMEM((3, slots, part), BF),
+            pltpu.VMEM((2, slots, part), BF),
+            pltpu.VMEM((2, slots // 2, part), BF),
+            pltpu.VMEM((2, slots // 2, part), BF),
             pltpu.VMEM((slots, part), BF),
             pltpu.VMEM((slots, part), BF),
             pltpu.VMEM((slots, hid), BF),
@@ -533,17 +596,24 @@
             pltpu.VMEM((width, hid), F32),
             pltpu.VMEM((width, hid), F32),
             pltpu.VMEM((hid, width), F32),
-            dma((4,)),
-            dma((3,)),
+            pltpu.VMEM((tokens, part), BF),
+            pltpu.VMEM((tokens, chan), BF),
+            pltpu.VMEM((tokens, chan), BF),
+            pltpu.VMEM((tokens, chan), BF),
+            pltpu.VMEM((block, chan), F32),
+            dma((9,)),
+            dma((8,)),
         ]
-        + [dma((8,))] * 12
+        + [dma((8,))] * 2
+        + [dma((16,))]
+        + [dma((8,))] * 14
         + [dma((2,))] * 6
         + [dma((5,))] * 2
         + [dma((8,))] * 2,
         compiler_params=pltpu.CompilerParams(
             collective_id=0, has_side_effects=True, vmem_limit_bytes=62 * 1024 * 1024
         ),
-    )(choice, scale, cot, stream, gain, og, ig, ci, taps, wg, wu, wd, ow)
+    )(choice, scale, gain, taps, stream, cot, ig, ci, og, wg, wu, wd, ow)
 
 
 def finish_kernel(*refs):
@@ -583,7 +653,7 @@
 ):
     sp_size = lax.axis_size("sp")
     arrays = whole_step(
-        expert_choice.T, route_scale.T, cotangent, stream_in, norm_gain[None], out_gate, in_gate, conv_input, conv_taps,
+        expert_choice.T, route_scale.T, norm_gain[None], conv_taps, stream_in, cotangent, in_gate, conv_input, out_gate,
         expert_gate[0], expert_up[0], expert_down[0], out_weight, sp_size,
     )
     *others, grad_gate, grad_up, grad_down = finished_outputs(arrays, 4)

time: 164 us -> 153 us (0.933)
  Pallas kernels: 163 us -> 152 us
    pallas_call x1, Pallas kernels: 158 us -> 147 us  [whole_step(): pl.pallas_call(functools.partial(step_kernel, plane), name='experts', out...]
where the time goes in v4:
time: 153 us
  Pallas kernels  152 us (99%)
    pallas_call x1, Pallas kernels, whole_step(): pl.pallas_call(functools.partial(step_kernel, plane), name='experts', out...  147 us
    pallas_call x1, Pallas kernels, finished_outputs(): pl.pallas_call(finish_kernel, name='finish', grid=(steps,), out_shape=[ja...  5.37 us

profile of v4, /device:TPU:1, one launch (start us, length us, event | category | flops | bytes accessed | tf_op | source)
XLA Modules:
  0.0 152.7 jit_solution(773402559026128598)
XLA Ops:
  0.6 146.7 %experts.1 = (bf16[256,512]{1,0:T(8,128)(2,1)}, bf16[256,256]{1,0:T(8,128)(2,1)}, bf16[256,256]{1,0:T(8,128)(2,1)}, bf16[256,256]{1,0:T(8,128)(2,1)}, f32[32,256...) custom-call(s32[2,256]{1,0:T(2,128)} %bitcast.13, ...), custom_call_target="tpu_custom_call" | custom-call | tf_op jit(solution)/shard_map/experts/pallas_call | solution.py:542
  147.3 5.4 %finish.1 = (bf16[256,512]{1,0:T(8,128)(2,1)}, bf16[256,256]{1,0:T(8,128)(2,1)}, bf16[256,256]{1,0:T(8,128)(2,1)}, bf16[256,256]{1,0:T(8,128)(2,1)}, f32[32,256]...) custom-call(bf16[256,512]{1,0:T(8,128)(2,1)} %get-tuple-element.24.refs_0_, ...), custom_call_target="tpu_custom_call" | custom-call | tf_op jit(solution)/shard_map/finish/pallas_call | solution.py:629

commit v5 on v4

--- a/solution.py
+++ b/solution.py
@@ -53,12 +53,12 @@
     (
         stream, cot, ig, ci, og, wg, wu, wd, ow, inverse, normed, pick, weight, send_all, send_part, rows, partial, summand, far_in, far_sum, total, back,
         hidden, ggrad, ugrad, gate_out, up_out, down_out, tok, sgrad, extended, filtered, mixed, fgrad,
-        owp, pair, psum, arrived, gate_sum, up_sum, down_sum,
+        owp, pair, psum, row_in, row_total, arrived, gate_sum, up_sum, down_sum,
         stream_out, og_out, ig_out, ci_out, ow_out,
         in_sem, out_sem,
         a_send, a_recv, half_recv, right_send, left_send, from_left, from_right,
         fright_send, fleft_send, ffrom_left, ffrom_right,
-        rs_send, far_send, of_left_recv, of_right_recv, far_left_recv, far_right_recv, tright_send, tleft_send, tfrom_left, tfrom_right, tf_send, tf_recv, one_send, one_recv, pair_send, pair_recv,
+        rs_send, far_send, of_left_recv, of_right_recv, far_left_recv, far_right_recv, tright_send, tleft_send, tfrom_left, tfrom_right, tf_send, tf_recv, one_send, one_recv, pair_send, pair_recv, row_send, row_recv,
     ) = refs
     me = lax.axis_index("sp")
     q = lax.axis_index("tp")
@@ -396,14 +396,14 @@
     wait_for(tok.at[high, of_far], tf_recv.at[1])
 
     def stream_rows(r):
-        at = rows_at(r, 16)
+        at = rows_at(r, 32)
         inv = inverse[at, :]
         unit = stream[at, :].astype(F32) * inv
         unit_grad = tok[at, :].astype(F32) * gain[...]
         along = jnp.mean(unit * unit_grad, axis=-1, keepdims=True)
         sgrad[at, :] = (cot[at, :].astype(F32) + inv * (unit_grad - unit * along)).astype(BF)
 
-    loop(0, tokens // 16, stream_rows)
+    loop(0, tokens // 32, stream_rows)
 
     block = width // experts
     pairs = experts // 2
@@ -412,6 +412,8 @@
     groups = plane // 2
     cut = plane * block
 
+    line = lax.rem(here, groups)
+
     def plane_of(j):
         half = lax.div(j + 1, 2)
         return lax.rem(z + 4 + half - 2 * half * lax.rem(j, 2), 8)
@@ -432,16 +434,14 @@
         psum[of_plane] = (owp[of_plane, core].astype(F32) + pair[of_plane].astype(F32)).astype(BF)
 
         def send_sum(k):
-            to = at * groups + lax.rem(here + k, groups)
-
-            @pl.when(to != here)
-            def _():
-                copy_to(psum.at[to], arrived.at[here], one_send.at[4], one_recv.at[4], 2 * to + core, q)
-
-        loop(0, groups, send_sum)
+            to = lax.rem(line + k, groups)
+            copy_to(
+                psum.at[at * groups + to], row_in.at[k - 1, at], row_send, row_recv.at[j], 2 * (z * groups + to) + core, q
+            )
+
+        loop(1, groups, send_sum)
 
     loop(0, 8, pair_sum)
-    arrived[here] = psum[here]
 
     mixed_grad = product_of(sgrad[...], ow[...])
     fgrad[0:tokens, :] = mixed_grad * og[...].astype(F32)
@@ -454,6 +454,21 @@
     def _():
         fgrad[tokens : tokens + 8, :] = jnp.zeros((8, part_of(fgrad)), F32)
 
+    def row_sum(j):
+        at = plane_of(j)
+        found = psum[at * groups + line].astype(F32)
+        if groups > 1:
+            wait_for(row_in.at[:, at], row_recv.at[j])
+            for k in range(groups - 1):
+                found = found + row_in[k, at].astype(F32)
+        row_total[at] = found.astype(BF)
+
+        @pl.when(at != z)
+        def _():
+            copy_to(row_total.at[at], arrived.at[z], one_send.at[4], one_recv.at[4], 2 * (at * groups + line) + core, q)
+
+    loop(0, 8, row_sum)
+    arrived[z] = row_total[z]
     og_out[...] = (mixed_grad * filtered[...]).astype(BF)
     finished[1].start()
     stream_out[...] = sgrad[:, mine]
@@ -504,6 +519,8 @@
         wait_for(pair.at[pl.ds(0, groups)], pair_send.at[j])
 
     loop(0, 8, pair_sent)
+    if groups > 1:
+        wait_for(psum.at[pl.ds(0, 8 * (groups - 1))], row_send)
 
     @pl.when(me < experts - 1)
     def _():
@@ -513,15 +530,15 @@
     def _():
         wait_for(fgrad.at[0:8], one_send.at[3])
 
-    wait_for(arrived.at[pl.ds(0, pairs - 1)], one_recv.at[4])
+    wait_for(arrived.at[pl.ds(0, 7)], one_recv.at[4])
     added = arrived[0].astype(F32)
-    for p in range(1, pairs):
+    for p in range(1, 8):
         added = added + arrived[p].astype(F32)
     ow_out[...] = added
     finished[4].start()
     for copy in finished:
         copy.wait()
-    wait_for(arrived.at[pl.ds(0, pairs - 1)], one_send.at[4])
+    wait_for(arrived.at[pl.ds(0, 7)], one_send.at[4])
 
 
 def part_of(ref):
@@ -592,7 +609,9 @@
             pltpu.VMEM((experts // 2, 2, block, chan), BF),
             pltpu.VMEM((experts // 2, block, chan), BF),
             pltpu.VMEM((experts // 2, block, chan), BF),
-            pltpu.VMEM((experts // 2, block, chan), BF),
+            pltpu.VMEM((max(1, plane // 2 - 1), 8, block, chan), BF),
+            pltpu.VMEM((8, block, chan), BF),
+            pltpu.VMEM((8, block, chan), BF),
             pltpu.VMEM((width, hid), F32),
             pltpu.VMEM((width, hid), F32),
             pltpu.VMEM((hid, width), F32),
@@ -609,30 +628,52 @@
         + [dma((8,))] * 14
         + [dma((2,))] * 6
         + [dma((5,))] * 2
-        + [dma((8,))] * 2,
+        + [dma((8,))] * 2
+        + [dma, dma((8,))],
         compiler_params=pltpu.CompilerParams(
             collective_id=0, has_side_effects=True, vmem_limit_bytes=62 * 1024 * 1024
         ),
     )(choice, scale, gain, taps, stream, cot, ig, ci, og, wg, wu, wd, ow)
 
 
-def finish_kernel(*refs):
-    half = len(refs) // 2
-    for given, out in zip(refs[:half], refs[half:]):
-        out[...] = given[...].astype(out.dtype)
-
-
-def finished_outputs(arrays, steps):
+def finish_kernel(pieces, *refs):
+    given, outs, held, wide, in_sem, out_sem = refs[:8], refs[8:16], refs[16:24], refs[24:27], refs[27], refs[28]
+
+    def cut(k):
+        rows = given[k].shape[0] // pieces
+        return [pl.ds(n * rows, rows) for n in range(pieces)] if k > 4 else [pl.ds(0, given[k].shape[0])]
+
+    order = [(k, at) for k in (5, 6, 7, 0, 1, 2, 3, 4) for at in cut(k)]
+    arriving = [pltpu.make_async_copy(given[k].at[at], held[k].at[at], in_sem.at[n]) for n, (k, at) in enumerate(order)]
+    leaving = [
+        pltpu.make_async_copy(wide[k - 5].at[at] if k > 4 else held[k].at[at], outs[k].at[at], out_sem.at[n])
+        for n, (k, at) in enumerate(order)
+    ]
+    for copy in arriving:
+        copy.start()
+    for (k, at), copy, then in zip(order, arriving, leaving):
+        copy.wait()
+        if k > 4:
+            wide[k - 5][at] = held[k][at].astype(F32)
+        then.start()
+    for copy in leaving:
+        copy.wait()
+
+
+def finished_outputs(arrays, pieces):
     types = [F32 if k > 3 else BF for k in range(len(arrays))]
-    specs = [pl.BlockSpec((a.shape[0] // steps, a.shape[1]), lambda i: (i, 0)) for a in arrays]
-    specs[4] = pl.BlockSpec(arrays[4].shape, lambda i: (0, 0))
+    hbm = pl.BlockSpec(memory_space=pltpu.HBM)
+    count = 5 + 3 * pieces
     return pl.pallas_call(
-        finish_kernel,
+        functools.partial(finish_kernel, pieces),
         name="finish",
-        grid=(steps,),
         out_shape=[jax.ShapeDtypeStruct(a.shape, t) for a, t in zip(arrays, types)],
-        in_specs=specs,
-        out_specs=specs,
+        in_specs=[hbm] * 8,
+        out_specs=[hbm] * 8,
+        scratch_shapes=[pltpu.VMEM(a.shape, a.dtype) for a in arrays]
+        + [pltpu.VMEM(a.shape, F32) for a in arrays[5:]]
+        + [pltpu.SemaphoreType.DMA((count,)), pltpu.SemaphoreType.DMA((count,))],
+        compiler_params=pltpu.CompilerParams(vmem_limit_bytes=60 * 1024 * 1024),
     )(*arrays)
 
 

time: 153 us -> 146 us (0.954)
  Pallas kernels: 152 us -> 145 us
    pallas_call x1, Pallas kernels: 147 us -> 141 us  [whole_step(): pl.pallas_call(functools.partial(step_kernel, plane), name='experts', out...]
where the time goes in v5:
time: 146 us
  Pallas kernels  145 us (99%)
    pallas_call x1, Pallas kernels, whole_step(): pl.pallas_call(functools.partial(step_kernel, plane), name='experts', out...  141 us
    pallas_call x1, Pallas kernels, finished_outputs(): pl.pallas_call(functools.partial(finish_kernel, pieces), name='finish', o...  4.11 us

profile of v5, /device:TPU:1, one launch (start us, length us, event | category | flops | bytes accessed | tf_op | source)
XLA Modules:
  0.0 146.1 jit_solution(11271224477449006077)
XLA Ops:
  0.6 141.3 %experts.1 = (bf16[256,512]{1,0:T(8,128)(2,1)}, bf16[256,256]{1,0:T(8,128)(2,1)}, bf16[256,256]{1,0:T(8,128)(2,1)}, bf16[256,256]{1,0:T(8,128)(2,1)}, f32[32,256...) custom-call(s32[2,256]{1,0:T(2,128)} %bitcast.13, ...), custom_call_target="tpu_custom_call" | custom-call | tf_op jit(solution)/shard_map/experts/pallas_call | solution.py:559
  142.0 4.1 %finish.1 = (bf16[256,512]{1,0:T(8,128)(2,1)}, bf16[256,256]{1,0:T(8,128)(2,1)}, bf16[256,256]{1,0:T(8,128)(2,1)}, bf16[256,256]{1,0:T(8,128)(2,1)}, f32[32,256]...) custom-call(bf16[256,512]{1,0:T(8,128)(2,1)} %get-tuple-element.24.refs_0_, ...), custom_call_target="tpu_custom_call" | custom-call | tf_op jit(solution)/shard_map/finish/pallas_call | solution.py:667

commit v6 on v5

--- a/solution.py
+++ b/solution.py
@@ -330,7 +330,7 @@
             copy_to(partial.at[lower, of_right], summand.at[0, lower, :], rs_send.at[t], of_left_recv.at[t], me, right)
             copy_to(partial.at[upper, of_left], summand.at[1, upper, :], rs_send.at[t], of_right_recv.at[t], me, left)
 
-            @pl.when(t < 6)
+            @pl.when(t < 5)
             def _():
                 add_grads(at)
 
@@ -363,7 +363,7 @@
     def late_grads(t):
         add_grads(rows_at(source_at(t), span))
 
-    loop(6, 7, late_grads)
+    loop(5, 7, late_grads)
 
     wait_for(back.at[pl.ds(0, (experts - 1) * CAP), :], one_recv.at[1])
     tok[:, mine] = rows_product(pick[...], back[...]).astype(BF)

time: 146 us -> 145 us (level)
  no operation moved by 1% of the time
where the time goes in v6:
time: 145 us
  Pallas kernels  144 us (99%)
    pallas_call x1, Pallas kernels, whole_step(): pl.pallas_call(functools.partial(step_kernel, plane), name='experts', out...  140 us
    pallas_call x1, Pallas kernels, finished_outputs(): pl.pallas_call(functools.partial(finish_kernel, pieces), name='finish', o...  4.11 us

profile of v6, /device:TPU:1, one launch (start us, length us, event | category | flops | bytes accessed | tf_op | source)
XLA Modules:
  0.0 144.9 jit_solution(6526260222393316028)
XLA Ops:
  0.6 140.2 %experts.1 = (bf16[256,512]{1,0:T(8,128)(2,1)}, bf16[256,256]{1,0:T(8,128)(2,1)}, bf16[256,256]{1,0:T(8,128)(2,1)}, bf16[256,256]{1,0:T(8,128)(2,1)}, f32[32,256...) custom-call(s32[2,256]{1,0:T(2,128)} %bitcast.13, ...), custom_call_target="tpu_custom_call" | custom-call | tf_op jit(solution)/shard_map/experts/pallas_call | solution.py:559
  140.8 4.1 %finish.1 = (bf16[256,512]{1,0:T(8,128)(2,1)}, bf16[256,256]{1,0:T(8,128)(2,1)}, bf16[256,256]{1,0:T(8,128)(2,1)}, bf16[256,256]{1,0:T(8,128)(2,1)}, f32[32,256]...) custom-call(bf16[256,512]{1,0:T(8,128)(2,1)} %get-tuple-element.24.refs_0_, ...), custom_call_target="tpu_custom_call" | custom-call | tf_op jit(solution)/shard_map/finish/pallas_call | solution.py:667

commit v7 on v6

--- a/solution.py
+++ b/solution.py
@@ -261,15 +261,27 @@
         far_sum[1, held_at, :] = (partial[lower, of_left].astype(F32) + far_in[1, held_at, :].astype(F32)).astype(BF)
         copy_to(far_sum.at[1, held_at, :], summand.at[1, lower, :], rs_send.at[t], of_right_recv.at[t], me, left)
 
+    def pass_half(t, turn):
+        block = lax.rem(lax.div(place, side) + turn, 2)
+        piece = rows.at[:, rows_at(2 * source_at(t) + block, span // 2), mine]
+        wait_for(piece, half_recv.at[2 * t + turn])
+        copy_to(piece, piece, right_send.at[t], from_left.at[t], me, right)
+        copy_to(piece, piece, left_send.at[t], from_right.at[t], me, left)
+
     def step(i):
-        @pl.when((i >= 1) & (i < 6))
-        def _():
-            for turn in range(2):
-                block = lax.rem(lax.div(place, side) + turn, 2)
-                piece = rows.at[:, rows_at(2 * source_at(i) + block, span // 2), mine]
-                wait_for(piece, half_recv.at[2 * i + turn])
-                copy_to(piece, piece, right_send.at[i], from_left.at[i], me, right)
-                copy_to(piece, piece, left_send.at[i], from_right.at[i], me, left)
+        odd = lax.rem(i, 2)
+
+        @pl.when(i < 6)
+        def _():
+            @pl.when(odd == 1)
+            def _():
+                pass_half(i, 0)
+
+            @pl.when((odd == 1) & (i < 5))
+            def _():
+                pass_half(i + 1, 0)
+
+            pass_half(i, 1)
 
         @pl.when(i == 3)
         def _():

time: 145 us -> 145 us (level)
  no operation moved by 1% of the time
where the time goes in v7:
time: 145 us; the launch traced here: 144 us
  Pallas kernels  143 us (99%)
    pallas_call x1, Pallas kernels, whole_step(): pl.pallas_call(functools.partial(step_kernel, plane), name='experts', out...  139 us
    pallas_call x1, Pallas kernels, finished_outputs(): pl.pallas_call(functools.partial(finish_kernel, pieces), name='finish', o...  4.11 us

profile of v7, /device:TPU:1, one launch (start us, length us, event | category | flops | bytes accessed | tf_op | source)
XLA Modules:
  0.0 143.8 jit_solution(8663847625304838998)
XLA Ops:
  0.6 139.0 %experts.1 = (bf16[256,512]{1,0:T(8,128)(2,1)}, bf16[256,256]{1,0:T(8,128)(2,1)}, bf16[256,256]{1,0:T(8,128)(2,1)}, bf16[256,256]{1,0:T(8,128)(2,1)}, f32[32,256...) custom-call(s32[2,256]{1,0:T(2,128)} %bitcast.13, ...), custom_call_target="tpu_custom_call" | custom-call | tf_op jit(solution)/shard_map/experts/pallas_call | solution.py:571
  139.7 4.1 %finish.1 = (bf16[256,512]{1,0:T(8,128)(2,1)}, bf16[256,256]{1,0:T(8,128)(2,1)}, bf16[256,256]{1,0:T(8,128)(2,1)}, bf16[256,256]{1,0:T(8,128)(2,1)}, f32[32,256]...) custom-call(bf16[256,512]{1,0:T(8,128)(2,1)} %get-tuple-element.24.refs_0_, ...), custom_call_target="tpu_custom_call" | custom-call | tf_op jit(solution)/shard_map/finish/pallas_call | solution.py:679
